TPU v7x, 32 devices: a whole 2x2x4 slice. The times are simulated.
32 devices in a mesh: grp: 2 (over y), sp: 8 (over z, core), tp: 2 (over x).
Axes of the slice: x: 2, y: 2, z: 4, core: 2. Of those that a mesh axis runs over, the one named last changes fastest.
Arguments:
- tokens: bfloat16 [12288, 2048], P(('grp', 'sp'), 'tp'), parts along dimension 0, may hold values from -4000 to 4000
- gain: float32 [2048], replicated, may hold values from 0.1 to 1.9
- w_query: bfloat16 [2048, 1024], P('sp', 'tp'), may hold values from -1 to 1
- w_key: bfloat16 [2048, 256], P('sp', 'tp'), may hold values from -1 to 1
- w_value: bfloat16 [2048, 256], P('sp', 'tp'), may hold values from -0.125 to 0.125
- w_input: bfloat16 [2048, 1024], P('sp', 'tp'), may hold values from -0.125 to 0.125
- w_bgate: bfloat16 [2048, 1024], P('sp', 'tp'), may hold values from -0.125 to 0.125
- w_cgate: bfloat16 [2048, 1024], P('sp', 'tp'), may hold values from -0.125 to 0.125
- w_attn_out: bfloat16 [1024, 2048], P('sp', 'tp'), may hold values from -2 to 2
- w_conv_out: bfloat16 [1024, 2048], P('sp', 'tp'), may hold values from -0.1875 to 0.1875
- sink_logit: float32 [16], P('tp'), may hold values from 0 to 5
- taps: float32 [3, 1024], P(None, 'tp'), may hold values from -3.5 to 3.5
- conv_bias: float32 [1024], P('tp'), may hold values from -4 to 4
- documents: int32 [12288], P(('grp', 'sp')), parts along dimension 0, may hold values from 0 to 3, never falling along the last dimension, each value on 1 to 3072 neighbouring positions
Outputs:
- mixed: bfloat16 [12288, 2048], P(('grp', 'sp'), 'tp'), parts along dimension 0
There are 2 independent parts, one for each index of `grp`. A program takes and returns all parts, laid end to end along the dimension named above; an argument that names none is the same for every part. Nothing has to cross between parts.
All inputs are finite; a program needn't handle non-finite values.
Results may differ from a plain program's by a relative error of at most 0.013.
The roundings to bfloat16 on the way count: a program that leaves them out, or rounds other values in their place, can miss the bound.
Values may be sent and summed in bfloat16 or wider, within the bound.
A program may use at most 64 MiB of HBM per device.

v0:
```python
import jax
import jax.numpy as jnp
from jax import lax
from jax.sharding import PartitionSpec as P

HEAD_DIM = 64
WINDOW = 128


EPS = 1e-06
THETA = 500000.0


def extended(cells, sides, width):
    for axis, dim in sides:
        count = lax.axis_size(axis)
        ends = count - 1
        head = lax.slice_in_dim(cells, 0, width, axis=dim)
        tail = lax.slice_in_dim(cells, cells.shape[dim] - width, cells.shape[dim], axis=dim)
        cells = jnp.concatenate(
            [
                lax.ppermute(tail, axis, [(i, (i + 1) % count) for i in range(ends)]),
                cells,
                lax.ppermute(head, axis, [((i + 1) % count, i) for i in range(ends)]),
            ],
            axis=dim,
        )
    return cells


def rotate(proj, positions, heads):
    rows = proj.shape[0]
    size = proj.shape[1] // heads
    half = size // 2
    freq = jnp.power(THETA, -(jnp.arange(half, dtype=jnp.float32) * (2.0 / size)))
    angle = positions.astype(jnp.float32)[:, None] * freq[None, :]
    cosine = jnp.cos(angle)[:, None, :]
    sine = jnp.sin(angle)[:, None, :]
    shaped = proj.reshape(rows, heads, size)
    first = shaped[..., :half]
    second = shaped[..., half:]
    turned = jnp.concatenate(
        [first * cosine - second * sine, second * cosine + first * sine], axis=-1
    )
    return turned.reshape(rows, heads * size)


def sink_softmax(scores, allowed, sinks):
    masked = jnp.where(allowed, scores, -jnp.inf)
    top = jnp.maximum(jnp.max(masked, axis=-1, keepdims=True), sinks)
    expo = jnp.exp(masked - top)
    return expo / (jnp.sum(expo, axis=-1, keepdims=True) + jnp.exp(sinks - top))


def local(
    tokens,
    gain,
    w_query,
    w_key,
    w_value,
    w_input,
    w_bgate,
    w_cgate,
    w_attn_out,
    w_conv_out,
    sink_logit,
    taps,
    conv_bias,
    documents,
):
    f32 = jnp.float32
    bf16 = jnp.bfloat16
    rows, part = tokens.shape
    tp_count = lax.axis_size("tp")
    sp_count = lax.axis_size("sp")
    width = part * tp_count
    head_dim = HEAD_DIM
    q_local = w_query.shape[1] // head_dim
    kv_local = w_key.shape[1] // head_dim
    groups = q_local // kv_local
    wq, wk, wv, wu, wb, wc, w_attn, w_conv = (
        lax.all_gather(w_query, "sp", axis=0, tiled=True),
        lax.all_gather(w_key, "sp", axis=0, tiled=True),
        lax.all_gather(w_value, "sp", axis=0, tiled=True),
        lax.all_gather(w_input, "sp", axis=0, tiled=True),
        lax.all_gather(w_bgate, "sp", axis=0, tiled=True),
        lax.all_gather(w_cgate, "sp", axis=0, tiled=True),
        lax.all_gather(w_attn_out, "sp", axis=0, tiled=True),
        lax.all_gather(w_conv_out, "sp", axis=0, tiled=True),
    )
    matrices = (wq, wk, wv, wu, wb, wc)
    piece_f = lax.all_gather(tokens, "tp", axis=1, tiled=True).astype(f32)
    scaled = (piece_f * gain[None, :]).astype(bf16)
    products = tuple((jnp.dot(scaled, mat, preferred_element_type=f32) for mat in matrices))
    folded = products + (jnp.sum(piece_f * piece_f, axis=1),)
    sums = folded[:6]
    squares = folded[6]
    inv = lax.rsqrt(squares / width + EPS)[:, None]
    q_acc, k_acc, v_acc, u_acc, b_acc, c_acc = sums
    positions = lax.axis_index("sp") * rows + jnp.arange(rows, dtype=jnp.int32)
    query = rotate(q_acc * inv, positions, q_local).astype(bf16)
    keys = rotate(k_acc * inv, positions, kv_local).astype(bf16)
    values = (v_acc * inv).astype(bf16)
    carried = (c_acc * inv * (u_acc * inv)).astype(bf16)
    bgate = b_acc * inv
    doc_col = documents.astype(f32).astype(bf16)[:, None]
    paired = jnp.concatenate([keys, values], axis=1)
    pair_ext, doc_ext = (
        extended(paired, (("sp", 0),), WINDOW),
        extended(doc_col, (("sp", 0),), WINDOW),
    )
    carry_ext, doc_near = (extended(carried, (("sp", 0),), 1), extended(doc_col, (("sp", 0),), 1))
    key_width = kv_local * head_dim
    key_ext = pair_ext[:, :key_width].reshape(-1, kv_local, head_dim)
    val_ext = pair_ext[:, key_width:].reshape(-1, kv_local, head_dim)
    key_doc = doc_ext[:, 0].astype(f32)
    own_doc = doc_col[:, 0].astype(f32)
    key_pos = positions[0] - WINDOW + jnp.arange(rows + 2 * WINDOW, dtype=jnp.int32)
    total = sp_count * rows
    sinks = sink_logit.reshape(kv_local, groups, 1, 1)
    block = rows // 2
    outputs = []
    for begin in range(0, rows, block):
        span = block + 2 * WINDOW
        q_block = query[begin : begin + block].reshape(block, kv_local, groups, head_dim)
        k_block = key_ext[begin : begin + span]
        v_block = val_ext[begin : begin + span]
        q_pos = positions[begin : begin + block]
        k_pos = key_pos[begin : begin + span]
        scores = jnp.einsum(
            "qhgd,khd->hgqk", q_block, k_block, preferred_element_type=f32
        ) * head_dim ** (-0.5)
        allowed = jnp.abs(q_pos[:, None] - k_pos[None, :]) <= WINDOW
        allowed = allowed & (
            own_doc[begin : begin + block, None] == key_doc[None, begin : begin + span]
        )
        allowed = allowed & (k_pos >= 0)[None, :] & (k_pos < total)[None, :]
        weight = sink_softmax(scores, allowed, sinks).astype(bf16)
        result = jnp.einsum("hgqk,khd->qhgd", weight, v_block, preferred_element_type=f32)
        outputs.append(result.astype(bf16).reshape(block, q_local * head_dim))
    attended = jnp.concatenate(outputs, axis=0)
    near_doc = doc_near[:, 0].astype(f32)
    conv = jnp.zeros((rows, carried.shape[1]), f32)
    for tap in range(3):
        same = (near_doc[tap : tap + rows] == near_doc[1 : rows + 1])[:, None]
        conv = conv + jnp.where(
            same, carry_ext[tap : tap + rows].astype(f32) * taps[tap][None, :], 0.0
        )
    convolved = (bgate * (conv + conv_bias[None, :])).astype(bf16)
    acc = jnp.dot(
        lax.all_gather(attended, "tp", axis=1, tiled=True), w_attn, preferred_element_type=f32
    )
    mixed = acc + jnp.dot(
        lax.all_gather(convolved, "tp", axis=1, tiled=True), w_conv, preferred_element_type=f32
    )
    return mixed.astype(bf16)


def solution(mesh):
    placed = (
        P(("grp", "sp"), "tp"),
        P(),
        P("sp", "tp"),
        P("sp", "tp"),
        P("sp", "tp"),
        P("sp", "tp"),
        P("sp", "tp"),
        P("sp", "tp"),
        P("sp", "tp"),
        P("sp", "tp"),
        P("tp"),
        P(None, "tp"),
        P("tp"),
        P(("grp", "sp")),
    )
    return jax.shard_map(
        local, mesh=mesh, in_specs=placed, out_specs=P(("grp", "sp"), "tp"), check_vma=False
    )
```

profile of v0, /device:TPU:0, one launch (start us, length us, event | category | flops | bytes accessed | tf_op | source)
XLA Modules:
  0.0 308.4 jit_solution(10480472641820720276)
XLA Ops:
  6.5 0.7 all-gather.10.cloned.1.call-update
  7.3 0.7 all-gather.12.cloned.1.call-update
  8.1 0.7 all-gather.20.cloned.1.call-update
  8.8 0.5 all-gather.22.cloned.1.call-update
  9.4 0.5 all-gather.18.cloned.1.call-update
  10.0 0.7 convert_convert_fusion
  10.7 1.3 collective-permute-start.2
  12.0 3.0 collective-permute-start.1
  15.1 0.5 slice.161
  16.3 17.1 %all_gather.35 = bf16[2048,128]{1,0:T(8,128)(2,1)S(1)} all-gather(bf16[256,128]{1,0:T(8,128)(2,1)} %param.18), channel_id=1, replica_groups=mesh['grp'=2,'sp'=8,'tp'=2] {'sp'}, dimensions={0}, use_global_device_ids=true | all-gather | bytes 589824 | tf_op jit(solution)/shard_map/all_gather | solution.py:84
  33.4 14.7 %all_gather.34 = bf16[2048,128]{1,0:T(8,128)(2,1)S(1)} all-gather(bf16[256,128]{1,0:T(8,128)(2,1)S(1)} %copy-done.3), channel_id=1, replica_groups=mesh['grp'=2,'sp'=8,'tp'=2] {'sp'}, dimensions={0}, use_global_device_ids=true | all-gather | bytes 589824 | tf_op jit(solution)/shard_map/all_gather | solution.py:83
  48.7 0.7 fusion.32
  49.4 7.1 %all-gather.10.cloned.1.call-done = bf16[768,2048]{1,0:T(8,128)(2,1)} async-done(((bf16[768,1024]{1,0:T(8,128)(2,1)}), bf16[768,2048]{1,0:T(8,128)(2,1)}) %all-gather.10.cloned.1.call-update) | async-done | bytes 3145744 | tf_op jit(solution)/shard_map/all_gather | solution.py:92
  56.5 2.7 fusion.3
  59.4 1.2 fusion.20
  60.7 1.2 fusion.26
  61.9 1.6 collective-permute-start
  63.5 1.5 collective-permute-start.3
  65.0 0.7 fusion.34
  65.7 2.3 collective-permute-done.3
  68.1 19.9 %all-gather.12.cloned.1.call-done = bf16[2048,512]{1,0:T(8,128)(2,1)} async-done(((bf16[256,512]{1,0:T(8,128)(2,1)}), bf16[2048,512]{1,0:T(8,128)(2,1)}) %all-gather.12.cloned.1.call-update) | async-done | bytes 2097168 | tf_op jit(solution)/shard_map/all_gather | solution.py:82
  88.0 4.4 %convolution_multiply_fusion = f32[768,512]{0,1:T(8,128)S(1)} fusion(bf16[2048,512]{1,0:T(8,128)(2,1)} %all-gather.12.cloned.1.call-done, bf16[768,2048]{1,0:T(8,128)(2,1)} %all-gather.10.cloned.1.call-done, f32[2048]{0:T(1024)S(1)} %copy-done.5, f32[768]{0:T(1024)S(1)} %add_rsqrt_fusion), kind=kOutput, calls=%fused_computation.19 | convolution fusion | flops 1615724544 | bytes 6827008 | tf_op jit(solution)/shard_map/dot_general | solution.py:94
  92.7 1.4 fusion.4
  94.2 1.6 fusion
  95.8 1.4 fusion.5
  97.3 1.7 fusion.1
  99.0 2.6 fusion.18
  101.6 2.6 fusion.19
  104.1 1.0 pad_maximum_fusion.2
  105.2 0.7 all-gather.26.cloned.1.call-update
  105.9 0.6 fusion.45
  106.5 1.3 collective-permute-start.5
  107.8 3.6 %collective-permute-start.4 = (bf16[1,1]{0,1:T(2,128)(2,1)}, bf16[1,1]{0,1:T(2,128)(2,1)}, u32[]{:S(2)}, u32[]{:S(2)}) collective-permute-start(bf16[1,1]{0,1:T(2,128)(2,1)} %bitcast.26), channel_id=1, source_target_pairs={{0,2},{2,4},{4,6},{6,8},{8,10},{10,12},{12,14},{1,3},{3,5},{5,7},{... | collective-permute-start | bytes 14 | tf_op jit(solution)/shard_map/ppermute | solution.py:22
  111.8 1.4 maximum_convert_fusion.1
  113.2 5.0 %all-gather.20.cloned.1.call-done = bf16[2048,512]{1,0:T(8,128)(2,1)} async-done(((bf16[256,512]{1,0:T(8,128)(2,1)}), bf16[2048,512]{1,0:T(8,128)(2,1)}) %all-gather.20.cloned.1.call-update) | async-done | bytes 2097168 | tf_op jit(solution)/shard_map/all_gather | solution.py:87
  118.2 5.5 %fusion.9 = f32[768,512]{0,1:T(8,128)} fusion(bf16[2048,512]{1,0:T(8,128)(2,1)} %all-gather.20.cloned.1.call-done, bf16[768,2048]{1,0:T(8,128)(2,1)} %all-gather.10.cloned.1.call-done, f32[2048]{0:T(1024)S(1)} %copy-done.5), kind=kOutput, calls=%fused_computation.20 | convolution fusion | flops 1615331328 | bytes 6823936 | tf_op jit(solution)/shard_map/dot_general | solution.py:94
  123.7 24.5 %all-gather.22.cloned.1.call-done = bf16[2048,512]{1,0:T(8,128)(2,1)} async-done(((bf16[256,512]{1,0:T(8,128)(2,1)}), bf16[2048,512]{1,0:T(8,128)(2,1)}) %all-gather.22.cloned.1.call-update) | async-done | bytes 2097168 | tf_op jit(solution)/shard_map/all_gather | solution.py:85
  148.2 3.9 %multiply_convert_fusion.1 = bf16[768,512]{0,1:T(8,128)(2,1)S(1)} fusion(f32[768,512]{0,1:T(8,128)} %fusion.9, bf16[2048,512]{1,0:T(8,128)(2,1)} %all-gather.22.cloned.1.call-done, bf16[768,2048]{1,0:T(8,128)(2,1)S(1)} %copy-done.1, f32[2048]{0:T(1024)S(1)} %copy-done.5, f32[768]{0:T(1024)S(1)} %add_rsqrt_fusion), kind=kOutput, calls=%fused_computation.18 | convolution fusion | flops 1616904192 | bytes 7613440 | tf_op jit(solution)/shard_map/dot_general | solution.py:94
  152.3 1.3 collective-permute-start.7
  153.6 3.7 %collective-permute-start.6 = (bf16[1,512]{0,1:T(8,128)(2,1)S(1)}, bf16[1,512]{0,1:T(8,128)(2,1)}, u32[]{:S(2)}, u32[]{:S(2)}) collective-permute-start(bf16[1,512]{0,1:T(8,128)(2,1)S(1)} %get-tuple-element.12), channel_id=1, source_target_pairs={{0,2},{2,4},{4,6},{6,8},{8,10},{10,12},{12,14},{1,3},{3,5},{5,7},{... | collective-permute-start | bytes 3080 | tf_op jit(solution)/shard_map/ppermute | solution.py:22
  157.4 20.9 %all-gather.18.cloned.1.call-done = bf16[2048,512]{1,0:T(8,128)(2,1)} async-done(((bf16[256,512]{1,0:T(8,128)(2,1)}), bf16[2048,512]{1,0:T(8,128)(2,1)}) %all-gather.18.cloned.1.call-update) | async-done | bytes 2097168 | tf_op jit(solution)/shard_map/all_gather | solution.py:86
  178.3 5.7 %multiply_convert_fusion = bf16[768,512]{0,1:T(8,128)(2,1)} fusion(bf16[768,512]{0,1:T(8,128)(2,1)} %copy-done.2, bf16[1,512]{0,1:T(8,128)(2,1)} %collective-permute-done.7, bf16[1,512]{0,1:T(8,128)(2,1)} %collective-permute-done.6, f32[512]{0:T(512)S(1)} %copy-done.6, f32[512]{0:T(512)S(1)} %bitcast.92, f32[512]{0:T(512)S(1)} %bitcast.93, ...), kind=kOutput, calls=%fused_computation.17 | convolution fusion | flops 1623588864 | bytes 6839552 | tf_op jit(solution)/shard_map/dot_general | solution.py:94
  184.0 25.7 %all-gather.16.cloned.1.call-done = bf16[1024,1024]{1,0:T(8,128)(2,1)} async-done(((bf16[128,1024]{1,0:T(8,128)(2,1)}), bf16[1024,1024]{1,0:T(8,128)(2,1)}) %all-gather.16.cloned.1.call-update) | async-done | bytes 2097168 | tf_op jit(solution)/shard_map/all_gather | solution.py:88
  209.7 28.1 %all-gather.14.cloned.1.call-done = bf16[768,1024]{0,1:T(8,128)(2,1)} async-done(((bf16[768,512]{0,1:T(8,128)(2,1)}), bf16[768,1024]{0,1:T(8,128)(2,1)}) %all-gather.14.cloned.1.call-update) | async-done | bytes 1572880 | tf_op jit(solution)/shard_map/all_gather | solution.py:151
  237.8 3.9 %fusion.47 = f32[768,1024]{1,0:T(8,128)S(1)} fusion(bf16[768,1024]{0,1:T(8,128)(2,1)} %all-gather.14.cloned.1.call-done, bf16[1024,1024]{1,0:T(8,128)(2,1)} %all-gather.16.cloned.1.call-done), kind=kOutput, calls=%fused_computation.92 | convolution fusion | flops 1610612736 | bytes 6815744 | tf_op jit(solution)/shard_map/dot_general | solution.py:150
  241.7 26.9 %all-gather.26.cloned.1.call-done = bf16[1024,1024]{1,0:T(8,128)(2,1)} async-done(((bf16[128,1024]{1,0:T(8,128)(2,1)}), bf16[1024,1024]{1,0:T(8,128)(2,1)}) %all-gather.26.cloned.1.call-update) | async-done | bytes 2097168 | tf_op jit(solution)/shard_map/all_gather | solution.py:89
  268.6 28.2 %all-gather.24.cloned.1.call-done = bf16[768,1024]{0,1:T(8,128)(2,1)} async-done(((bf16[768,512]{0,1:T(8,128)(2,1)}), bf16[768,1024]{0,1:T(8,128)(2,1)}) %all-gather.24.cloned.1.call-update) | async-done | bytes 1572880 | tf_op jit(solution)/shard_map/all_gather | solution.py:154
  296.8 5.0 %add_convert_fusion = bf16[768,1024]{1,0:T(8,128)(2,1)} fusion(f32[768,1024]{1,0:T(8,128)S(1)} %fusion.47, bf16[768,1024]{0,1:T(8,128)(2,1)} %all-gather.24.cloned.1.call-done, bf16[1024,1024]{1,0:T(8,128)(2,1)} %all-gather.26.cloned.1.call-done), kind=kOutput, calls=%fused_computation.16 | convolution fusion | flops 1612185600 | bytes 8388608 | tf_op jit(solution)/shard_map/dot_general | solution.py:153
  (61 shorter events, 2.4 us)
Async XLA Ops:
  6.5 26.9 %copy-start.3 = (bf16[256,128]{1,0:T(8,128)(2,1)S(1)}, bf16[256,128]{1,0:T(8,128)(2,1)}, u32[]{:S(2)}) copy-start(bf16[256,128]{1,0:T(8,128)(2,1)} %param.17) | copy-start | bytes 196612
  6.5 42.0 %copy-start.7 = (f32[8]{0:T(128)S(1)}, f32[8]{0:T(128)}, u32[]{:S(2)}) copy-start(f32[8]{0:T(128)} %param.24) | copy-start | bytes 100
  6.5 50.0 %all-gather.10.cloned.1.call-start = ((), (), s32[]{:S(2)}) async-start(), calls=%async_computation | async-start | bytes 4718592 | tf_op jit(solution)/shard_map/all_gather | solution.py:92
  7.3 52.0 %copy-start.5 = (f32[2048]{0:T(1024)S(1)}, f32[2048]{0:T(1024)}, u32[]{:S(2)}) copy-start(f32[2048]{0:T(1024)} %param.15) | copy-start | bytes 24580
  7.3 80.8 %all-gather.12.cloned.1.call-start = ((), (), s32[]{:S(2)}) async-start(), calls=%async_computation.1 | async-start | bytes 2359296 | tf_op jit(solution)/shard_map/all_gather | solution.py:82
  8.0 110.2 %all-gather.20.cloned.1.call-start = ((), (), s32[]{:S(2)}) async-start(), calls=%async_computation.5 | async-start | bytes 2359296 | tf_op jit(solution)/shard_map/all_gather | solution.py:87
  8.8 139.5 %all-gather.22.cloned.1.call-start = ((), (), s32[]{:S(2)}) async-start(), calls=%async_computation.6 | async-start | bytes 2359296 | tf_op jit(solution)/shard_map/all_gather | solution.py:85
  9.3 168.9 %all-gather.18.cloned.1.call-start = ((), (), s32[]{:S(2)}) async-start(), calls=%async_computation.4 | async-start | bytes 2359296 | tf_op jit(solution)/shard_map/all_gather | solution.py:86
  9.9 199.8 %all-gather.16.cloned.1.call-start = ((), (), s32[]{:S(2)}) async-start(), calls=%async_computation.3 | async-start | bytes 2359296 | tf_op jit(solution)/shard_map/all_gather | solution.py:88
  10.7 38.0 %collective-permute-start.2 = (bf16[128,1]{0,1:T(2,128)(2,1)S(1)}, bf16[128,1]{0,1:T(2,128)(2,1)S(1)}, u32[]{:S(2)}, u32[]{:S(2)}) collective-permute-start(bf16[128,1]{0,1:T(2,128)(2,1)S(1)} %get-tuple-element.44), channel_id=1, source_target_pairs={{2,0},{4,2},{6,4},{8,6},{10,8},{12,10},{14,12},{3,1},{5,3},{7,5},{... | collective-permute-start | bytes 776 | tf_op jit(solution)/shard_map/ppermute | solution.py:24
  12.0 36.7 %collective-permute-start.1 = (bf16[128,1]{0,1:T(2,128)(2,1)S(1)}, bf16[128,1]{0,1:T(2,128)(2,1)S(1)}, u32[]{:S(2)}, u32[]{:S(2)}) collective-permute-start(bf16[128,1]{0,1:T(2,128)(2,1)S(1)} %get-tuple-element.43), channel_id=1, source_target_pairs={{0,2},{2,4},{4,6},{6,8},{8,10},{10,12},{12,14},{1,3},{3,5},{5,7},{... | collective-permute-start | bytes 776 | tf_op jit(solution)/shard_map/ppermute | solution.py:22
  15.0 222.8 %all-gather.14.cloned.1.call-start = ((), (), s32[]{:S(2)}) async-start(), calls=%async_computation.2 | async-start | bytes 2359296 | tf_op jit(solution)/shard_map/all_gather | solution.py:151
  56.5 2.8 copy-start
  61.9 3.8 %collective-permute-start = (bf16[128,256]{0,1:T(8,128)(2,1)S(1)}, bf16[128,256]{0,1:T(8,128)(2,1)S(1)}, u32[]{:S(2)}, u32[]{:S(2)}) collective-permute-start(bf16[128,256]{0,1:T(8,128)(2,1)S(1)} %get-tuple-element.24), channel_id=1, source_target_pairs={{0,2},{2,4},{4,6},{6,8},{8,10},{10,12},{12,14},{1,3},{3,5},{5,7},{... | collective-permute-start | bytes 196616 | tf_op jit(solution)/shard_map/ppermute | solution.py:22
  63.5 4.6 %collective-permute-start.3 = (bf16[128,256]{0,1:T(8,128)(2,1)S(1)}, bf16[128,256]{0,1:T(8,128)(2,1)S(1)}, u32[]{:S(2)}, u32[]{:S(2)}) collective-permute-start(bf16[128,256]{0,1:T(8,128)(2,1)S(1)} %get-tuple-element.25), channel_id=1, source_target_pairs={{2,0},{4,2},{6,4},{8,6},{10,8},{12,10},{14,12},{3,1},{5,3},{7,5},{... | collective-permute-start | bytes 196616 | tf_op jit(solution)/shard_map/ppermute | solution.py:24
  101.6 9.9 %copy-start.4 = (f32[3,512]{1,0:T(4,128)S(1)}, f32[3,512]{1,0:T(4,128)}, u32[]{:S(2)}) copy-start(f32[3,512]{1,0:T(4,128)} %param.25) | copy-start | bytes 18436
  105.1 163.5 %all-gather.26.cloned.1.call-start = ((), (), s32[]{:S(2)}) async-start(), calls=%async_computation.8 | async-start | bytes 2359296 | tf_op jit(solution)/shard_map/all_gather | solution.py:89
  105.9 190.9 %all-gather.24.cloned.1.call-start = ((), (), s32[]{:S(2)}) async-start(), calls=%async_computation.7 | async-start | bytes 2359296 | tf_op jit(solution)/shard_map/all_gather | solution.py:154
  106.5 4.9 %collective-permute-start.5 = (bf16[1,1]{0,1:T(2,128)(2,1)}, bf16[1,1]{0,1:T(2,128)(2,1)}, u32[]{:S(2)}, u32[]{:S(2)}) collective-permute-start(bf16[1,1]{0,1:T(2,128)(2,1)} %bitcast.27), channel_id=1, source_target_pairs={{2,0},{4,2},{6,4},{8,6},{10,8},{12,10},{14,12},{3,1},{5,3},{7,5},{... | collective-permute-start | bytes 14 | tf_op jit(solution)/shard_map/ppermute | solution.py:24
  107.8 4.0 %collective-permute-start.4 = (bf16[1,1]{0,1:T(2,128)(2,1)}, bf16[1,1]{0,1:T(2,128)(2,1)}, u32[]{:S(2)}, u32[]{:S(2)}) collective-permute-start(bf16[1,1]{0,1:T(2,128)(2,1)} %bitcast.26), channel_id=1, source_target_pairs={{0,2},{2,4},{4,6},{6,8},{8,10},{10,12},{12,14},{1,3},{3,5},{5,7},{... | collective-permute-start | bytes 14 | tf_op jit(solution)/shard_map/ppermute | solution.py:22
  113.2 35.0 %copy-start.1 = (bf16[768,2048]{1,0:T(8,128)(2,1)S(1)}, bf16[768,2048]{1,0:T(8,128)(2,1)}, u32[]{:S(2)}) copy-start(bf16[768,2048]{1,0:T(8,128)(2,1)} %all-gather.10.cloned.1.call-done) | copy-start | bytes 9437188
  123.7 54.5 %copy-start.6 = (f32[512]{0:T(512)S(1)}, f32[512]{0:T(512)}, u32[]{:S(2)}) copy-start(f32[512]{0:T(512)} %param.26) | copy-start | bytes 6148
  152.1 5.1 %copy-start.2 = (bf16[768,512]{0,1:T(8,128)(2,1)}, bf16[768,512]{0,1:T(8,128)(2,1)S(1)}, u32[]{:S(2)}) copy-start(bf16[768,512]{0,1:T(8,128)(2,1)S(1)} %multiply_convert_fusion.1) | copy-start | bytes 2359300
  152.3 26.0 %collective-permute-start.7 = (bf16[1,512]{0,1:T(8,128)(2,1)S(1)}, bf16[1,512]{0,1:T(8,128)(2,1)}, u32[]{:S(2)}, u32[]{:S(2)}) collective-permute-start(bf16[1,512]{0,1:T(8,128)(2,1)S(1)} %get-tuple-element.13), channel_id=1, source_target_pairs={{2,0},{4,2},{6,4},{8,6},{10,8},{12,10},{14,12},{3,1},{5,3},{7,5},{... | collective-permute-start | bytes 3080 | tf_op jit(solution)/shard_map/ppermute | solution.py:24
  153.6 24.7 %collective-permute-start.6 = (bf16[1,512]{0,1:T(8,128)(2,1)S(1)}, bf16[1,512]{0,1:T(8,128)(2,1)}, u32[]{:S(2)}, u32[]{:S(2)}) collective-permute-start(bf16[1,512]{0,1:T(8,128)(2,1)S(1)} %get-tuple-element.12), channel_id=1, source_target_pairs={{0,2},{2,4},{4,6},{6,8},{8,10},{10,12},{12,14},{1,3},{3,5},{5,7},{... | collective-permute-start | bytes 3080 | tf_op jit(solution)/shard_map/ppermute | solution.py:22
Sparse Core Ops, SparseCore 0:
  8.9 47.6 all-gather.9
  58.1 29.8 all-gather.11
  89.6 28.5 all-gather.19
  119.7 28.5 all-gather.21
  149.7 28.5 all-gather.17
  179.7 29.9 all-gather.15
  211.2 26.5 all-gather.13
  239.4 29.1 all-gather.25
  270.2 26.5 all-gather.23
where the time goes:
time: 309 us; the launch traced here: 308 us
  waiting for transfers between devices  193 us (62%)
  matrix products  38.7 us (13%)
  blocking collectives  31.8 us (10%)
  starting transfers between devices  17.6 us (6%)
  between operations  14.2 us (5%)
  other arithmetic  11.9 us (4%)
    all_gather x1, waiting for transfers between devices, local(): lax.all_gather(convolved, 'tp', axis=1, tiled=True)  28.2 us
    all_gather x1, waiting for transfers between devices, local(): lax.all_gather(attended, 'tp', axis=1, tiled=True)  28.1 us
    all_gather x1, waiting for transfers between devices, local(): lax.all_gather(w_conv_out, 'sp', axis=0, tiled=True)  26.9 us
    all_gather x1, waiting for transfers between devices, local(): lax.all_gather(w_attn_out, 'sp', axis=0, tiled=True)  25.7 us
    all_gather x1, waiting for transfers between devices, local(): lax.all_gather(w_input, 'sp', axis=0, tiled=True)  24.5 us
    dot_general x6, matrix products, local(): jnp.dot(scaled, mat, preferred_element_type=f32)  21.9 us
    all_gather x1, waiting for transfers between devices, local(): lax.all_gather(w_bgate, 'sp', axis=0, tiled=True)  20.9 us
    all_gather x1, waiting for transfers between devices, local(): lax.all_gather(w_query, 'sp', axis=0, tiled=True)  19.9 us
  transfers between devices with their start and end apart: 17, of which 11 were waited for; matrix products, arithmetic and copies ran while one was open for 15% of the time, Pallas kernels for 0%

commit v1 on v0

--- a/solution.py
+++ b/solution.py
@@ -1,6 +1,10 @@
+import functools
+
 import jax
 import jax.numpy as jnp
 from jax import lax
+from jax.experimental import pallas as pl
+from jax.experimental.pallas import tpu as pltpu
 from jax.sharding import PartitionSpec as P
 
 HEAD_DIM = 64
@@ -9,6 +13,328 @@
 
 EPS = 1e-06
 THETA = 500000.0
+PROJ_UNITS = 4
+OUT_UNITS = 2
+TOKEN_CHUNKS = 4
+
+
+def fused_plan(grp_count, sp_count, tp_count, rows, part, proj_rows, out_rows):
+    lines = sp_count // 2
+    return (
+        grp_count == 2
+        and tp_count == 2
+        and sp_count % 2 == 0
+        and 2 <= lines <= 4
+        and proj_rows % (2 * PROJ_UNITS * 16) == 0
+        and out_rows % (2 * OUT_UNITS * 16) == 0
+        and rows % (TOKEN_CHUNKS * 16) == 0
+        and part % 128 == 0
+    )
+
+
+def gather_kernel(
+    sizes,
+    tok_ref,
+    gain_ref,
+    wp_ref,
+    wo_ref,
+    proj_ref,
+    wo_full,
+    wp_full,
+    tok_other,
+    scaled,
+    inv_ref,
+    z_send,
+    z_recv,
+    y_send,
+    y_recv,
+    dz_send,
+    dz_recv,
+    dy_send,
+    dy_recv,
+    do_send,
+    do_recv,
+    x_send,
+    x_recv,
+    own_sem,
+):
+    lines, cut = sizes
+    f32 = jnp.float32
+    rows, part = tok_ref.shape
+    rp = wp_ref.shape[0]
+    ro = wo_ref.shape[0]
+    up, uo = rp // 2 // PROJ_UNITS, ro // 2 // OUT_UNITS
+    y = lax.axis_index("grp")
+    sp = lax.axis_index("sp")
+    x = lax.axis_index("tp")
+    z, c = sp // 2, sp % 2
+    proj_units = list(range(PROJ_UNITS))
+    out_units = list(range(PROJ_UNITS, PROJ_UNITS + OUT_UNITS))
+    to_y = {"grp": 1 - y}
+    to_core = {"sp": z * 2 + 1 - c}
+    to_x = {"tp": 1 - x}
+    to_z = ({"sp": sp + 2}, {"sp": sp - 2})
+    has_next = (z < lines - 1, z > 0)
+
+    def origin(way, t):
+        return z - t if way == 0 else z + t
+
+    def arrives(way, t):
+        return z >= t if way == 0 else z < lines - t
+
+    def place(u, zo, cc, h):
+        if u < PROJ_UNITS:
+            row = (zo * 2 + cc) * rp + h * (rp // 2) + u * up
+            return wp_full.at[pl.ds(pl.multiple_of(row, up), up), :]
+        row = (zo * 2 + cc) * ro + h * (ro // 2) + (u - PROJ_UNITS) * uo
+        return wo_full.at[pl.ds(pl.multiple_of(row, uo), uo), :]
+
+    def mine(u, h):
+        if u < PROJ_UNITS:
+            row = h * (rp // 2) + u * up
+            return wp_ref.at[pl.ds(pl.multiple_of(row, up), up), :]
+        row = h * (ro // 2) + (u - PROJ_UNITS) * uo
+        return wo_ref.at[pl.ds(pl.multiple_of(row, uo), uo), :]
+
+    def remote(src, dst, send, recv, device):
+        return pltpu.make_async_remote_copy(
+            src_ref=src, dst_ref=dst, send_sem=send, recv_sem=recv,
+            device_id=device, device_id_type=pl.DeviceIdType.MESH,
+        )
+
+    def z_copy(way, t, u):
+        zo = origin(way, t)
+        dst = place(u, zo, c, y)
+        src = mine(u, y) if t == 0 else dst
+        return remote(src, dst, z_send.at[way, t, u], z_recv.at[way, t, u], to_z[way])
+
+    def z_arrival(way, t, u):
+        dst = place(u, origin(way, t), c, y)
+        return remote(dst, dst, z_send.at[way, t - 1, u], z_recv.at[way, t - 1, u], to_z[way])
+
+    def y_copy(way, t, u):
+        ref = place(u, origin(way, t), c, y)
+        return remote(ref, ref, y_send.at[way, t - 1, u], y_recv.at[way, t - 1, u], to_y)
+
+    def y_arrival(way, t, u):
+        ref = place(u, origin(way, t), c, 1 - y)
+        return remote(ref, ref, y_send.at[way, t - 1, u], y_recv.at[way, t - 1, u], to_y)
+
+    def d_copy(kind, way, t, u, cc):
+        send, recv = (dz_send, dz_recv) if kind == 0 else (dy_send, dy_recv)
+        ref = place(u, origin(way, t), cc, y if kind == 0 else 1 - y)
+        return remote(ref, ref, send.at[way, t - 1, u], recv.at[way, t - 1, u], to_core)
+
+    def own_d(group, cc):
+        ref, full, size = (wp_ref, wp_full, rp) if group == 0 else (wo_ref, wo_full, ro)
+        dst = full.at[pl.ds(pl.multiple_of((z * 2 + cc) * size, size), size), :]
+        return remote(ref, dst, do_send.at[group], do_recv.at[group], to_core)
+
+    def own_local(group):
+        ref, full, size = (wp_ref, wp_full, rp) if group == 0 else (wo_ref, wo_full, ro)
+        dst = full.at[pl.ds(pl.multiple_of((z * 2 + c) * size, size), size), :]
+        return pltpu.make_async_copy(ref, dst, own_sem.at[group])
+
+    chunk = rows // TOKEN_CHUNKS
+
+    def x_copy(k):
+        return remote(
+            tok_ref.at[pl.ds(k * chunk, chunk), :], tok_other.at[pl.ds(k * chunk, chunk), :],
+            x_send.at[k], x_recv.at[k], to_x,
+        )
+
+    barrier = pltpu.get_barrier_semaphore()
+    for device in (to_y, to_core, to_x):
+        pl.semaphore_signal(barrier, inc=1, device_id=device, device_id_type=pl.DeviceIdType.MESH)
+    for way in range(2):
+
+        @pl.when(has_next[way])
+        def _():
+            pl.semaphore_signal(
+                barrier, inc=1, device_id=to_z[way], device_id_type=pl.DeviceIdType.MESH
+            )
+
+    neighbours = jnp.where(z > 0, 1, 0) + jnp.where(z < lines - 1, 1, 0) + 3
+    pl.semaphore_wait(barrier, neighbours)
+
+    def start_own(units):
+        for u in units:
+            for way in range(2):
+
+                @pl.when(has_next[way])
+                def _():
+                    z_copy(way, 0, u).start()
+
+    start_own(proj_units)
+    for k in range(TOKEN_CHUNKS):
+        x_copy(k).start()
+    own_d(0, c).start()
+    own_local(0).start()
+
+    def event(t, u):
+        for way in range(2):
+
+            @pl.when(arrives(way, t))
+            def _():
+                z_arrival(way, t, u).wait_recv()
+                if t < lines - 1:
+
+                    @pl.when(has_next[way])
+                    def _():
+                        z_copy(way, t, u).start()
+
+                y_copy(way, t, u).start()
+                d_copy(0, way, t, u, c).start()
+
+    def y_event(t, u):
+        for way in range(2):
+
+            @pl.when(arrives(way, t))
+            def _():
+                y_arrival(way, t, u).wait_recv()
+                d_copy(1, way, t, u, c).start()
+
+    def scale(k):
+        x_copy(k).wait_recv()
+        tile = 32
+
+        def body(i, carry):
+            at = pl.ds(pl.multiple_of(k * chunk + i * tile, tile), tile)
+            own = tok_ref[at, :].astype(f32)
+            other = tok_other[at, :].astype(f32)
+            total = jnp.sum(own * own, axis=1, keepdims=True) + jnp.sum(
+                other * other, axis=1, keepdims=True
+            )
+            inv_ref[at, :] = jnp.broadcast_to(
+                lax.rsqrt(total / (2 * part) + EPS), (tile, inv_ref.shape[1])
+            )
+            mine_at = pl.multiple_of(x * part, part)
+            other_at = pl.multiple_of((1 - x) * part, part)
+            scaled[at, pl.ds(mine_at, part)] = (own * gain_ref[:, pl.ds(mine_at, part)]).astype(
+                scaled.dtype
+            )
+            scaled[at, pl.ds(other_at, part)] = (
+                other * gain_ref[:, pl.ds(other_at, part)]
+            ).astype(scaled.dtype)
+            return carry
+
+        lax.fori_loop(0, chunk // tile, body, 0)
+
+    steps = [(t, u) for t in range(1, lines) for u in proj_units]
+    done = 0
+    for i, (t, u) in enumerate(steps):
+        event(t, u)
+        if i >= 1:
+            y_event(*steps[i - 1])
+        if (t, u) == (lines - 1, 0):
+            start_own(out_units)
+            own_d(1, c).start()
+            own_local(1).start()
+        while done < TOKEN_CHUNKS - 1 and (i + 1) * TOKEN_CHUNKS >= (done + 1) * len(steps):
+            scale(done)
+            done += 1
+    y_event(*steps[-1])
+    while done < TOKEN_CHUNKS:
+        scale(done)
+        done += 1
+    own_d(0, 1 - c).wait_recv()
+    own_local(0).wait()
+    for t, u in steps:
+        for way in range(2):
+
+            @pl.when(arrives(way, t))
+            def _():
+                d_copy(0, way, t, u, 1 - c).wait_recv()
+                d_copy(1, way, t, u, 1 - c).wait_recv()
+
+    width = proj_ref.shape[1]
+    blocks = width // cut
+    tail = [(t, u) for t in range(1, lines) for u in out_units]
+    cuts = [blocks * i // len(tail) for i in range(len(tail) + 1)]
+
+    def project(begin, end):
+        def body(j, carry):
+            at = pl.ds(pl.multiple_of(j * cut, cut), cut)
+            acc = jnp.dot(scaled[...], wp_full[:, at], preferred_element_type=f32)
+            proj_ref[:, at] = acc * inv_ref[:, :1]
+            return carry
+
+        lax.fori_loop(begin, end, body, 0)
+
+    for i, (t, u) in enumerate(tail):
+        project(cuts[i], cuts[i + 1])
+        event(t, u)
+        if i >= 1:
+            y_event(*tail[i - 1])
+    y_event(*tail[-1])
+    own_d(1, 1 - c).wait_recv()
+    own_local(1).wait()
+    for t, u in tail:
+        for way in range(2):
+
+            @pl.when(arrives(way, t))
+            def _():
+                d_copy(0, way, t, u, 1 - c).wait_recv()
+                d_copy(1, way, t, u, 1 - c).wait_recv()
+
+    for group in range(2):
+        own_d(group, c).wait_send()
+    for k in range(TOKEN_CHUNKS):
+        x_copy(k).wait_send()
+    for u in proj_units + out_units:
+        for way in range(2):
+
+            @pl.when(has_next[way])
+            def _():
+                z_copy(way, 0, u).wait_send()
+
+            for t in range(1, lines):
+
+                @pl.when(arrives(way, t))
+                def _():
+                    if t < lines - 1:
+
+                        @pl.when(has_next[way])
+                        def _():
+                            z_copy(way, t, u).wait_send()
+
+                    y_copy(way, t, u).wait_send()
+                    d_copy(0, way, t, u, c).wait_send()
+                    d_copy(1, way, t, u, c).wait_send()
+
+
+def gather_project(tokens, gain, w_proj, w_out, sp_count):
+    rows, part = tokens.shape
+    lines = sp_count // 2
+    width = w_proj.shape[1]
+    cut = 256 if width % 256 == 0 else 128
+    units = PROJ_UNITS + OUT_UNITS
+    dma = pltpu.SemaphoreType.DMA
+    hops = (2, lines - 1, units)
+    vmem = pl.BlockSpec(memory_space=pltpu.VMEM)
+    flops = 2 * rows * 2 * part * width
+    return pl.pallas_call(
+        functools.partial(gather_kernel, (lines, cut)),
+        out_shape=(
+            jax.ShapeDtypeStruct((rows, width), jnp.float32),
+            jax.ShapeDtypeStruct((w_out.shape[0] * sp_count, w_out.shape[1]), w_out.dtype),
+        ),
+        in_specs=[vmem] * 4,
+        out_specs=(vmem, pl.BlockSpec(memory_space=pl.ANY)),
+        scratch_shapes=[
+            pltpu.VMEM((w_proj.shape[0] * sp_count, width), w_proj.dtype),
+            pltpu.VMEM((rows, part), tokens.dtype),
+            pltpu.VMEM((rows, 2 * part), jnp.bfloat16),
+            pltpu.VMEM((rows, 128), jnp.float32),
+        ]
+        + [dma(hops)] * 8
+        + [dma((2,)), dma((2,)), dma((TOKEN_CHUNKS,)), dma((TOKEN_CHUNKS,)), dma((2,))],
+        compiler_params=pltpu.CompilerParams(
+            collective_id=0, has_side_effects=True, vmem_limit_bytes=60 * 1024 * 1024
+        ),
+        cost_estimate=pl.CostEstimate(flops=flops, bytes_accessed=0, transcendentals=0),
+        name="gather_project",
+    )(tokens, gain[None, :], w_proj, w_out)
 
 
 def extended(cells, sides, width):
@@ -78,25 +404,45 @@
     q_local = w_query.shape[1] // head_dim
     kv_local = w_key.shape[1] // head_dim
     groups = q_local // kv_local
-    wq, wk, wv, wu, wb, wc, w_attn, w_conv = (
-        lax.all_gather(w_query, "sp", axis=0, tiled=True),
-        lax.all_gather(w_key, "sp", axis=0, tiled=True),
-        lax.all_gather(w_value, "sp", axis=0, tiled=True),
-        lax.all_gather(w_input, "sp", axis=0, tiled=True),
-        lax.all_gather(w_bgate, "sp", axis=0, tiled=True),
-        lax.all_gather(w_cgate, "sp", axis=0, tiled=True),
-        lax.all_gather(w_attn_out, "sp", axis=0, tiled=True),
-        lax.all_gather(w_conv_out, "sp", axis=0, tiled=True),
-    )
-    matrices = (wq, wk, wv, wu, wb, wc)
-    piece_f = lax.all_gather(tokens, "tp", axis=1, tiled=True).astype(f32)
-    scaled = (piece_f * gain[None, :]).astype(bf16)
-    products = tuple((jnp.dot(scaled, mat, preferred_element_type=f32) for mat in matrices))
-    folded = products + (jnp.sum(piece_f * piece_f, axis=1),)
-    sums = folded[:6]
-    squares = folded[6]
-    inv = lax.rsqrt(squares / width + EPS)[:, None]
-    q_acc, k_acc, v_acc, u_acc, b_acc, c_acc = sums
+    if fused_plan(
+        lax.axis_size("grp"), sp_count, tp_count, rows, part, w_query.shape[0], w_attn_out.shape[0]
+    ):
+        cols = (w_query, w_key, w_value, w_input, w_bgate, w_cgate)
+        proj, w_both = gather_project(
+            tokens,
+            gain,
+            jnp.concatenate(cols, axis=1),
+            jnp.concatenate((w_attn_out, w_conv_out), axis=1),
+            sp_count,
+        )
+        parts, at = [], 0
+        for col in cols:
+            parts.append(proj[:, at : at + col.shape[1]])
+            at += col.shape[1]
+        q_acc, k_acc, v_acc, u_acc, b_acc, c_acc = parts
+        w_attn = w_both[:, :part]
+        w_conv = w_both[:, part:]
+        inv = jnp.float32(1.0)
+    else:
+        wq, wk, wv, wu, wb, wc, w_attn, w_conv = (
+            lax.all_gather(w_query, "sp", axis=0, tiled=True),
+            lax.all_gather(w_key, "sp", axis=0, tiled=True),
+            lax.all_gather(w_value, "sp", axis=0, tiled=True),
+            lax.all_gather(w_input, "sp", axis=0, tiled=True),
+            lax.all_gather(w_bgate, "sp", axis=0, tiled=True),
+            lax.all_gather(w_cgate, "sp", axis=0, tiled=True),
+            lax.all_gather(w_attn_out, "sp", axis=0, tiled=True),
+            lax.all_gather(w_conv_out, "sp", axis=0, tiled=True),
+        )
+        matrices = (wq, wk, wv, wu, wb, wc)
+        piece_f = lax.all_gather(tokens, "tp", axis=1, tiled=True).astype(f32)
+        scaled = (piece_f * gain[None, :]).astype(bf16)
+        products = tuple((jnp.dot(scaled, mat, preferred_element_type=f32) for mat in matrices))
+        folded = products + (jnp.sum(piece_f * piece_f, axis=1),)
+        sums = folded[:6]
+        squares = folded[6]
+        inv = lax.rsqrt(squares / width + EPS)[:, None]
+        q_acc, k_acc, v_acc, u_acc, b_acc, c_acc = sums
     positions = lax.axis_index("sp") * rows + jnp.arange(rows, dtype=jnp.int32)
     query = rotate(q_acc * inv, positions, q_local).astype(bf16)
     keys = rotate(k_acc * inv, positions, kv_local).astype(bf16)
@@ -147,12 +493,22 @@
             same, carry_ext[tap : tap + rows].astype(f32) * taps[tap][None, :], 0.0
         )
     convolved = (bgate * (conv + conv_bias[None, :])).astype(bf16)
-    acc = jnp.dot(
-        lax.all_gather(attended, "tp", axis=1, tiled=True), w_attn, preferred_element_type=f32
-    )
-    mixed = acc + jnp.dot(
-        lax.all_gather(convolved, "tp", axis=1, tiled=True), w_conv, preferred_element_type=f32
-    )
+    me = lax.axis_index("tp")
+    terms = []
+    for shift in range(tp_count):
+        hops = [(i, (i + shift) % tp_count) for i in range(tp_count)]
+        owner = (me + tp_count - shift) % tp_count
+        for mixer, weight in ((convolved, w_conv), (attended, w_attn)):
+            piece = mixer if shift == 0 else lax.ppermute(mixer, "tp", hops)
+            span = piece.shape[1]
+            terms.append(
+                jnp.dot(
+                    piece,
+                    lax.dynamic_slice_in_dim(weight, owner * span, span, 0),
+                    preferred_element_type=f32,
+                )
+            )
+    mixed = functools.reduce(jnp.add, terms)
     return mixed.astype(bf16)
 
 

time: 309 us -> 194 us (0.63)
  waiting for transfers between devices: 193 us -> 14 us
  Pallas kernels: 0 us -> 86.2 us
  blocking collectives: 31.8 us -> 0 us
  local copies, waits for them, and re-layouts: 1.46 us -> 26 us
  matrix products: 38.7 us -> 21.5 us
  between operations: 14.2 us -> 1.09 us
  other arithmetic: 11.9 us -> 23.2 us
  starting transfers between devices: 17.6 us -> 21.4 us
    all_gather x9 -> x0, waiting for transfers between devices: 186 us -> none  [the longest x1 28.2 us: local(): lax.all_gather(convolved, 'tp', axis=1, tiled=True)]
    pallas_call x0 -> x1, Pallas kernels: none -> 86.2 us  [gather_project(): pl.pallas_call(functools.partial(gather_kernel, (lines, cut)), out_shape=...]
    all_gather x2 -> x0, blocking collectives: 31.8 us -> none  [the longest x1 17.1 us: local(): lax.all_gather(w_value, 'sp', axis=0, tiled=True)]
    dot_general x8 -> x4, matrix products: 30.8 us -> 7.68 us  [local(): jnp.dot(piece, lax.dynamic_slice_in_dim(weight, owner * span, span, 0), p...]
    ppermute x0 -> x2, waiting for transfers between devices: none -> 14 us  [local(): piece = mixer if shift == 0 else lax.ppermute(mixer, 'tp', hops)]
    slice x0 -> x9, local copies, waits for them, and re-layouts: none -> 12.3 us  [the longest x4 5.41 us: local(): parts.append(proj[:, at:at + col.shape[1]])]
    unnamed x16 -> x45, local copies, waits for them, and re-layouts: 0.12 us -> 7.77 us
    dot_general x2, matrix products: 5.12 us -> 11.2 us  [local(): jnp.einsum('hgqk,khd->qhgd', weight, v_block, preferred_element_type=f32)]
  transfers between devices with their start and end apart: 17 -> 10, of which waited for: 11 -> 1; matrix products, arithmetic and copies ran while one was open for 15% -> 28% of each run, Pallas kernels for 0% -> 0%
where the time goes in v1:
time: 194 us; the launch traced here: 193 us
  Pallas kernels  86.2 us (44%)
  local copies, waits for them, and re-layouts  26 us (13%)
  other arithmetic  23.2 us (12%)
  matrix products  21.5 us (11%)
  starting transfers between devices  21.4 us (11%)
  waiting for transfers between devices  14 us (7%)
    pallas_call x1, Pallas kernels, gather_project(): pl.pallas_call(functools.partial(gather_kernel, (lines, cut)), out_shape=...  86.2 us
    ppermute x4, starting transfers between devices, extended(): lax.ppermute(tail, axis, [(i, (i + 1) % count) for i in range(ends)])  14 us
    ppermute x2, waiting for transfers between devices, local(): piece = mixer if shift == 0 else lax.ppermute(mixer, 'tp', hops)  14 us
    dot_general x2, matrix products, local(): jnp.einsum('hgqk,khd->qhgd', weight, v_block, preferred_element_type=f32)  11.2 us
    unnamed x45, local copies, waits for them, and re-layouts  7.77 us
    dot_general x4, matrix products, local(): jnp.dot(piece, lax.dynamic_slice_in_dim(weight, owner * span, span, 0), p...  7.68 us
    slice x4, local copies, waits for them, and re-layouts, local(): parts.append(proj[:, at:at + col.shape[1]])  5.41 us
    ppermute x4, starting transfers between devices, extended(): lax.ppermute(head, axis, [((i + 1) % count, i) for i in range(ends)])  5.28 us
  transfers between devices with their start and end apart: 10, of which 1 were waited for; matrix products, arithmetic and copies ran while one was open for 28% of the time, Pallas kernels for 0%

profile of v1, /device:TPU:0, one launch (start us, length us, event | category | flops | bytes accessed | tf_op | source)
XLA Modules:
  0.0 193.4 jit_solution(4993711234480197328)
XLA Ops:
  0.0 1.0 constant_dynamic-update-slice_fusion.5
  1.0 0.9 constant_dynamic-update-slice_fusion.4
  1.9 0.9 constant_dynamic-update-slice_fusion.3
  2.8 1.0 constant_dynamic-update-slice_fusion.2
  3.7 1.0 constant_dynamic-update-slice_fusion.1
  4.7 1.0 constant_dynamic-update-slice_fusion.wp_ref
  5.7 0.9 pad_maximum_fusion.3.wo_ref
  6.9 86.2 %gather_project.1 = (f32[768,2304]{1,0:T(8,128)}, bf16[1024,2048]{1,0:T(8,128)(2,1)}) custom-call(bf16[768,1024]{1,0:T(8,128)(2,1)} %tok_ref.1, f32[1,2048]{1,0:T(1,128)} %bitcast.89, bf16[256,2304]{1,0:T(8,128)(2,1)} %copy-done.13, bf16[128,2048]{1,0:T(8,128)(2,1)} %pad_maximum_fusion.3.wo_ref), custom_call_target="tpu_custom_call" | custom-call | flops 7247757312 | tf_op jit(solution)/shard_map/gather_project/pallas_call | solution.py:316
  93.1 3.9 %fusion.34 = (f32[768,512]{1,0:T(8,128)}, bf16[768,512]{1,0:T(8,128)(2,1)S(1)}) fusion(f32[768,2304]{1,0:T(8,128)} %get-tuple-element.7), kind=kLoop, calls=%fused_computation.93 | loop fusion | flops 786432 | bytes 7077888 | tf_op jit(solution)/shard_map/slice | solution.py:420
  97.6 1.3 collective-permute-start.3
  98.9 3.6 %collective-permute-start.2 = (bf16[1,512]{1,0:T(2,128)(2,1)}, bf16[1,512]{1,0:T(2,128)(2,1)}, u32[]{:S(2)}, u32[]{:S(2)}) collective-permute-start(bf16[1,512]{1,0:T(2,128)(2,1)} %get-tuple-element.22), channel_id=1, source_target_pairs={{0,2},{2,4},{4,6},{6,8},{8,10},{10,12},{12,14},{1,3},{3,5},{5,7},{... | collective-permute-start | bytes 3080 | tf_op jit(solution)/shard_map/ppermute | solution.py:348
  102.5 0.6 fusion.41
  103.1 1.3 collective-permute-start.1
  104.4 4.2 %collective-permute-start = (bf16[1,1]{0,1:T(2,128)(2,1)}, bf16[1,1]{0,1:T(2,128)(2,1)}, u32[]{:S(2)}, u32[]{:S(2)}) collective-permute-start(bf16[1,1]{0,1:T(2,128)(2,1)} %bitcast.1), channel_id=1, source_target_pairs={{0,2},{2,4},{4,6},{6,8},{8,10},{10,12},{12,14},{1,3},{3,5},{5,7},{... | collective-permute-start | bytes 14 | tf_op jit(solution)/shard_map/ppermute | solution.py:348
  108.6 1.0 slice.278
  109.7 1.1 slice.198
  111.7 0.7 pad_maximum_fusion.13
  112.4 3.1 %collective-permute-start.4 = (bf16[128,256]{1,0:T(8,128)(2,1)}, bf16[128,256]{1,0:T(8,128)(2,1)S(1)}, u32[]{:S(2)}, u32[]{:S(2)}) collective-permute-start(bf16[128,256]{1,0:T(8,128)(2,1)} %get-tuple-element.32), channel_id=1, source_target_pairs={{0,2},{2,4},{4,6},{6,8},{8,10},{10,12},{12,14},{1,3},{3,5},{5,7},{... | collective-permute-start | bytes 196616 | tf_op jit(solution)/shard_map/ppermute | solution.py:348
  117.3 0.6 slice_bitcast_fusion.1
  119.7 4.0 %fusion.35 = (bf16[1024,1024]{1,0:T(8,128)(2,1)S(1)}, bf16[1024,1024]{1,0:T(8,128)(2,1)}) fusion(bf16[1024,2048]{1,0:T(8,128)(2,1)} %get-tuple-element.8), kind=kLoop, calls=%fused_computation.94 | loop fusion | bytes 8388608 | tf_op jit(solution)/shard_map/slice | solution.py:423
  123.7 3.1 %copy.29 = f32[768,512]{0,1:T(8,128)} copy(f32[768,512]{1,0:T(8,128)} %get-tuple-element.14) | data formatting | bytes 3145728 | tf_op jit(solution)/shard_map/slice | solution.py:420
  126.8 2.3 %subtract_convert_fusion = (bf16[768,8,32]{0,2,1:T(8,128)(2,1)S(1)}, bf16[768,8,32]{0,2,1:T(8,128)(2,1)}) fusion(f32[768,8,64]{0,2,1:T(8,128)} %bitcast.73, f32[768,32]{0,1:T(8,128)S(1)} %get-tuple-element.38, f32[768,32]{0,1:T(8,128)S(1)} %get-tuple-element.37), kind=kLoop, calls=%fused_computation.39 | loop fusion | flops 1572864 | bytes 2555904 | tf_op jit(solution)/shard_map/convert
  129.1 0.7 max.32
  129.9 2.1 %fusion.24 = (bf16[384,8,64]{0,2,1:T(8,128)(2,1)}, bf16[384,8,64]{0,2,1:T(8,128)(2,1)}) fusion(bf16[768,8,32]{0,2,1:T(8,128)(2,1)S(1)} %get-tuple-element.18, bf16[768,8,32]{0,2,1:T(8,128)(2,1)} %get-tuple-element.19), kind=kLoop, calls=%fused_computation.41 | loop fusion | flops 1572864 | bytes 1572864 | tf_op jit(solution)/shard_map/concatenate | solution.py:368
  131.9 1.4 collective-permute-start.6
  133.4 3.0 %collective-permute-start.5 = (bf16[128,1]{0,1:T(2,128)(2,1)}, bf16[128,1]{0,1:T(2,128)(2,1)S(1)}, u32[]{:S(2)}, u32[]{:S(2)}) collective-permute-start(bf16[128,1]{0,1:T(2,128)(2,1)} %get-tuple-element.49), channel_id=1, source_target_pairs={{0,2},{2,4},{4,6},{6,8},{8,10},{10,12},{12,14},{1,3},{3,5},{5,7},{... | collective-permute-start | bytes 776 | tf_op jit(solution)/shard_map/ppermute | solution.py:348
  136.4 1.2 maximum_convert_fusion.1
  137.7 1.3 collective-permute-start.7
  139.1 1.6 fusion.21
  140.7 1.6 fusion.23
  142.4 3.5 %multiply_convert_fusion = bf16[768,512]{1,0:T(8,128)(2,1)} fusion(bf16[768,512]{1,0:T(8,128)(2,1)S(1)} %get-tuple-element.15, f32[768,2304]{1,0:T(8,128)} %get-tuple-element.7, bf16[1,512]{1,0:T(2,128)(2,1)} %collective-permute-done.3, bf16[1,512]{1,0:T(2,128)(2,1)} %collective-permute-done.2, f32[512]{0:T(512)S(1)} %copy-done.19, f32[512]{0:T(512)S(1)} %bitcast.87, ...), kind=kLoop, calls=%fused_computation.13 | loop fusion | flops 7864320 | bytes 3158272 | tf_op jit(solution)/shard_map/convert_element_type | solution.py:495
  145.8 1.5 collective-permute-start.8
  147.3 0.7 pad_maximum_fusion.9
  148.1 1.7 copy.31
  149.8 0.8 copy.32
  150.8 1.3 fusion.2
  152.2 1.6 fusion
  153.8 1.3 copy-done
  155.2 1.3 fusion.3
  156.6 1.6 fusion.1
  158.3 1.4 copy-done.1
  159.9 5.5 %fusion.6 = bf16[2,64,4,384]{3,1,2,0:T(8,128)(2,1)S(1)} fusion(bf16[640,2,64,1]{0,2,3,1:T(8,128)(2,1)S(1)} %bitcast.84, f32[2,640,384,4]{2,1,3,0:T(8,128)} %copy-done.1, f32[2,4,384]{2,1,0:T(4,128)S(1)} %exponential_add_fusion, f32[2,4,384]{2,1,0:T(4,128)S(1)} %get-tuple-element.54, pred[384,640]{0,1:T(8,128)(4,1)S(1)} %fusion.21), kind=kOutput, calls=%fused_computation.15 | convolution fusion | flops 261685248 | bytes 8691712 | tf_op jit(solution)/shard_map/hgqk,khd->qhgd/dot_general | solution.py:485
  165.4 5.6 %fusion.7 = bf16[2,64,4,384]{3,1,2,0:T(8,128)(2,1)S(1)} fusion(bf16[640,2,64,1]{0,2,3,1:T(8,128)(2,1)S(1)} %bitcast.85, f32[2,640,384,4]{2,1,3,0:T(8,128)} %copy-done, f32[2,4,384]{2,1,0:T(4,128)S(1)} %get-tuple-element.53, f32[2,4,384]{2,1,0:T(4,128)S(1)} %broadcast_maximum_fusion.1, pred[384,640]{0,1:T(8,128)(4,1)S(1)} %fusion.23), kind=kOutput, calls=%fused_computation.16 | convolution fusion | flops 261685248 | bytes 8691712 | tf_op jit(solution)/shard_map/hgqk,khd->qhgd/dot_general | solution.py:485
  171.7 2.1 %fusion.16 = f32[768,1024]{1,0:T(8,128)S(1)} fusion(bf16[768,512]{1,0:T(8,128)(2,1)} %multiply_convert_fusion, bf16[1024,1024]{1,0:T(8,128)(2,1)S(1)} %copy-done.2, s32[]{:T(128)S(6)} %select_n.40), kind=kOutput, calls=%fused_computation.23 | convolution fusion | flops 805306368 | bytes 4980740 | tf_op jit(solution)/shard_map/dot_general | solution.py:505
  173.9 1.0 fusion.14
  174.9 2.1 %fusion.12 = f32[768,1024]{1,0:T(8,128)S(1)} fusion(bf16[768,512]{1,0:T(8,128)(2,1)} %collective-permute-done.8, bf16[1024,1024]{1,0:T(8,128)(2,1)S(1)} %copy-done.2, s32[]{:T(128)S(6)} %select_n.44), kind=kOutput, calls=%fused_computation.19 | convolution fusion | flops 805306368 | bytes 4980740 | tf_op jit(solution)/shard_map/dot_general | solution.py:505
  177.0 14.0 %collective-permute-done.9 = bf16[768,512]{0,1:T(8,128)(2,1)S(1)} collective-permute-done((bf16[768,512]{0,1:T(8,128)(2,1)S(1)}, bf16[768,512]{0,1:T(8,128)(2,1)S(1)}, u32[]{:S(2)}, u32[]{:S(2)}) %collective-permute-start.9) | collective-permute-done | bytes 786464 | tf_op jit(solution)/shard_map/ppermute | solution.py:502
  191.0 2.4 %add_convert_fusion = bf16[768,1024]{1,0:T(8,128)(2,1)} fusion(f32[768,1024]{1,0:T(8,128)S(1)} %fusion.12, f32[768,1024]{1,0:T(8,128)S(1)} %fusion.16, f32[768,1024]{1,0:T(8,128)S(1)} %fusion.14, bf16[768,512]{0,1:T(8,128)(2,1)S(1)} %collective-permute-done.9, bf16[1024,1024]{1,0:T(8,128)(2,1)S(1)} %get-tuple-element.16, s32[]{:T(128)S(6)} %select_n.44), kind=kOutput, calls=%fused_computation.12 | convolution fusion | flops 808452096 | bytes 12845060 | tf_op jit(solution)/shard_map/dot_general | solution.py:505
  (74 shorter events, 6.0 us)
Async XLA Ops:
  0.0 5.7 %copy-start.10 = (bf16[128,1024]{1,0:T(8,128)(2,1)S(1)}, bf16[128,1024]{1,0:T(8,128)(2,1)}, u32[]{:S(2)}) copy-start(bf16[128,1024]{1,0:T(8,128)(2,1)} %param.23) | copy-start | bytes 786436
  0.0 5.7 %copy-start.11 = (bf16[128,1024]{1,0:T(8,128)(2,1)S(1)}, bf16[128,1024]{1,0:T(8,128)(2,1)}, u32[]{:S(2)}) copy-start(bf16[128,1024]{1,0:T(8,128)(2,1)} %param.22) | copy-start | bytes 786436
  5.7 1.2 copy-start.13
  93.1 9.4 %copy-start.18 = (s32[768]{0:T(1024)S(1)}, s32[768]{0:T(1024)}, u32[]{:S(2)}) copy-start(s32[768]{0:T(1024)} %param.27) | copy-start | bytes 9220
  97.6 44.7 %collective-permute-start.3 = (bf16[1,512]{1,0:T(2,128)(2,1)}, bf16[1,512]{1,0:T(2,128)(2,1)}, u32[]{:S(2)}, u32[]{:S(2)}) collective-permute-start(bf16[1,512]{1,0:T(2,128)(2,1)} %get-tuple-element.23), channel_id=1, source_target_pairs={{2,0},{4,2},{6,4},{8,6},{10,8},{12,10},{14,12},{3,1},{5,3},{7,5},{... | collective-permute-start | bytes 3080 | tf_op jit(solution)/shard_map/ppermute | solution.py:350
  98.9 43.4 %collective-permute-start.2 = (bf16[1,512]{1,0:T(2,128)(2,1)}, bf16[1,512]{1,0:T(2,128)(2,1)}, u32[]{:S(2)}, u32[]{:S(2)}) collective-permute-start(bf16[1,512]{1,0:T(2,128)(2,1)} %get-tuple-element.22), channel_id=1, source_target_pairs={{0,2},{2,4},{4,6},{6,8},{8,10},{10,12},{12,14},{1,3},{3,5},{5,7},{... | collective-permute-start | bytes 3080 | tf_op jit(solution)/shard_map/ppermute | solution.py:348
  103.1 28.8 %collective-permute-start.1 = (bf16[1,1]{0,1:T(2,128)(2,1)}, bf16[1,1]{0,1:T(2,128)(2,1)}, u32[]{:S(2)}, u32[]{:S(2)}) collective-permute-start(bf16[1,1]{0,1:T(2,128)(2,1)} %bitcast.2), channel_id=1, source_target_pairs={{2,0},{4,2},{6,4},{8,6},{10,8},{12,10},{14,12},{3,1},{5,3},{7,5},{... | collective-permute-start | bytes 14 | tf_op jit(solution)/shard_map/ppermute | solution.py:350
  104.4 28.9 %collective-permute-start = (bf16[1,1]{0,1:T(2,128)(2,1)}, bf16[1,1]{0,1:T(2,128)(2,1)}, u32[]{:S(2)}, u32[]{:S(2)}) collective-permute-start(bf16[1,1]{0,1:T(2,128)(2,1)} %bitcast.1), channel_id=1, source_target_pairs={{0,2},{2,4},{4,6},{6,8},{8,10},{10,12},{12,14},{1,3},{3,5},{5,7},{... | collective-permute-start | bytes 14 | tf_op jit(solution)/shard_map/ppermute | solution.py:348
  109.6 10.0 %copy-start.3 = (bf16[768,128]{1,0:T(8,128)(2,1)}, bf16[768,128]{1,0:T(8,128)(2,1)S(1)}, u32[]{:S(2)}) copy-start(bf16[768,128]{1,0:T(8,128)(2,1)S(1)} %slice.278) | copy-start | bytes 589828
  109.7 9.4 %copy-start.17 = (f32[3,512]{1,0:T(4,128)S(1)}, f32[3,512]{1,0:T(4,128)}, u32[]{:S(2)}) copy-start(f32[3,512]{1,0:T(4,128)} %param.25) | copy-start | bytes 18436
  111.6 8.0 %copy-start.5 = (bf16[768,128]{1,0:T(8,128)(2,1)}, bf16[768,128]{1,0:T(8,128)(2,1)S(1)}, u32[]{:S(2)}) copy-start(bf16[768,128]{1,0:T(8,128)(2,1)S(1)} %copy.26) | copy-start | bytes 589828
  112.4 35.0 %collective-permute-start.4 = (bf16[128,256]{1,0:T(8,128)(2,1)}, bf16[128,256]{1,0:T(8,128)(2,1)S(1)}, u32[]{:S(2)}, u32[]{:S(2)}) collective-permute-start(bf16[128,256]{1,0:T(8,128)(2,1)} %get-tuple-element.32), channel_id=1, source_target_pairs={{0,2},{2,4},{4,6},{6,8},{8,10},{10,12},{12,14},{1,3},{3,5},{5,7},{... | collective-permute-start | bytes 196616 | tf_op jit(solution)/shard_map/ppermute | solution.py:348
  129.1 13.2 %copy-start.14 = (f32[1,512]{1,0:T(1,128)S(1)}, f32[1,512]{1,0:T(1,128)}, u32[]{:S(2)}) copy-start(f32[1,512]{1,0:T(1,128)} %get-tuple-element.34) | copy-start | bytes 6148
  129.1 13.2 %copy-start.15 = (f32[1,512]{1,0:T(1,128)S(1)}, f32[1,512]{1,0:T(1,128)}, u32[]{:S(2)}) copy-start(f32[1,512]{1,0:T(1,128)} %get-tuple-element.35) | copy-start | bytes 6148
  129.1 13.2 %copy-start.16 = (f32[1,512]{1,0:T(1,128)S(1)}, f32[1,512]{1,0:T(1,128)}, u32[]{:S(2)}) copy-start(f32[1,512]{1,0:T(1,128)} %get-tuple-element.36) | copy-start | bytes 6148
  129.1 13.2 %copy-start.19 = (f32[512]{0:T(512)S(1)}, f32[512]{0:T(512)}, u32[]{:S(2)}) copy-start(f32[512]{0:T(512)} %param.26) | copy-start | bytes 6148
  131.9 15.4 %copy-start.4 = (bf16[768,128]{1,0:T(8,128)(2,1)S(1)}, bf16[768,128]{1,0:T(8,128)(2,1)}, u32[]{:S(2)}) copy-start(bf16[768,128]{1,0:T(8,128)(2,1)} %copy-done.3) | copy-start | bytes 589828
  131.9 15.4 %copy-start.6 = (bf16[768,128]{1,0:T(8,128)(2,1)S(1)}, bf16[768,128]{1,0:T(8,128)(2,1)}, u32[]{:S(2)}) copy-start(bf16[768,128]{1,0:T(8,128)(2,1)} %copy-done.5) | copy-start | bytes 589828
  131.9 5.8 %collective-permute-start.6 = (bf16[128,1]{0,1:T(2,128)(2,1)}, bf16[128,1]{0,1:T(2,128)(2,1)S(1)}, u32[]{:S(2)}, u32[]{:S(2)}) collective-permute-start(bf16[128,1]{0,1:T(2,128)(2,1)} %get-tuple-element.50), channel_id=1, source_target_pairs={{2,0},{4,2},{6,4},{8,6},{10,8},{12,10},{14,12},{3,1},{5,3},{7,5},{... | collective-permute-start | bytes 776 | tf_op jit(solution)/shard_map/ppermute | solution.py:350
  133.4 5.7 %collective-permute-start.5 = (bf16[128,1]{0,1:T(2,128)(2,1)}, bf16[128,1]{0,1:T(2,128)(2,1)S(1)}, u32[]{:S(2)}, u32[]{:S(2)}) collective-permute-start(bf16[128,1]{0,1:T(2,128)(2,1)} %get-tuple-element.49), channel_id=1, source_target_pairs={{0,2},{2,4},{4,6},{6,8},{8,10},{10,12},{12,14},{1,3},{3,5},{5,7},{... | collective-permute-start | bytes 776 | tf_op jit(solution)/shard_map/ppermute | solution.py:348
  137.7 9.6 %collective-permute-start.7 = (bf16[128,256]{1,0:T(8,128)(2,1)}, bf16[128,256]{1,0:T(8,128)(2,1)S(1)}, u32[]{:S(2)}, u32[]{:S(2)}) collective-permute-start(bf16[128,256]{1,0:T(8,128)(2,1)} %get-tuple-element.33), channel_id=1, source_target_pairs={{2,0},{4,2},{6,4},{8,6},{10,8},{12,10},{14,12},{3,1},{5,3},{7,5},{... | collective-permute-start | bytes 196616 | tf_op jit(solution)/shard_map/ppermute | solution.py:350
  145.8 5.0 %copy-start.8 = (bf16[384,8,64]{0,2,1:T(8,128)(2,1)S(1)}, bf16[384,8,64]{0,2,1:T(8,128)(2,1)}, u32[]{:S(2)}) copy-start(bf16[384,8,64]{0,2,1:T(8,128)(2,1)} %get-tuple-element.20) | copy-start | bytes 1179652
  145.8 29.1 %collective-permute-start.8 = (bf16[768,512]{1,0:T(8,128)(2,1)}, bf16[768,512]{1,0:T(8,128)(2,1)}, u32[]{:S(2)}, u32[]{:S(2)}) collective-permute-start(bf16[768,512]{1,0:T(8,128)(2,1)} %multiply_convert_fusion), channel_id=1, source_target_pairs={{0,1},{1,0},{2,3},{3,2},{4,5},{5,4},{6,7},{7,6},{8,9},{9,8},{10,11... | collective-permute-start | bytes 2359304 | tf_op jit(solution)/shard_map/ppermute | solution.py:502
  152.1 3.1 %copy-start = (f32[2,640,384,4]{2,1,3,0:T(8,128)}, f32[2,640,384,4]{2,1,3,0:T(8,128)S(1)}, u32[]{:S(2)}) copy-start(f32[2,640,384,4]{2,1,3,0:T(8,128)S(1)} %get-tuple-element.56) | copy-start | bytes 23592964
  152.2 3.0 %copy-start.7 = (bf16[384,8,64]{0,2,1:T(8,128)(2,1)S(1)}, bf16[384,8,64]{0,2,1:T(8,128)(2,1)}, u32[]{:S(2)}) copy-start(bf16[384,8,64]{0,2,1:T(8,128)(2,1)} %get-tuple-element.21) | copy-start | bytes 1179652
  152.2 3.0 %copy-start.9 = (bf16[640,128]{0,1:T(8,128)(2,1)S(1)}, bf16[640,128]{0,1:T(8,128)(2,1)}, u32[]{:S(2)}) copy-start(bf16[640,128]{0,1:T(8,128)(2,1)} %copy.32) | copy-start | bytes 491524
  156.5 3.1 %copy-start.1 = (f32[2,640,384,4]{2,1,3,0:T(8,128)}, f32[2,640,384,4]{2,1,3,0:T(8,128)S(1)}, u32[]{:S(2)}) copy-start(f32[2,640,384,4]{2,1,3,0:T(8,128)S(1)} %get-tuple-element.58) | copy-start | bytes 23592964
  156.6 3.3 %copy-start.12 = (bf16[640,128]{0,1:T(8,128)(2,1)S(1)}, bf16[640,128]{0,1:T(8,128)(2,1)}, u32[]{:S(2)}) copy-start(bf16[640,128]{0,1:T(8,128)(2,1)} %copy.31) | copy-start | bytes 491524
  165.4 6.3 %copy-start.2 = (bf16[1024,1024]{1,0:T(8,128)(2,1)S(1)}, bf16[1024,1024]{1,0:T(8,128)(2,1)}, u32[]{:S(2)}) copy-start(bf16[1024,1024]{1,0:T(8,128)(2,1)} %get-tuple-element.17) | copy-start | bytes 6291460
  171.1 19.9 %collective-permute-start.9 = (bf16[768,512]{0,1:T(8,128)(2,1)S(1)}, bf16[768,512]{0,1:T(8,128)(2,1)S(1)}, u32[]{:S(2)}, u32[]{:S(2)}) collective-permute-start(bf16[768,512]{0,1:T(8,128)(2,1)S(1)} %pad_maximum_fusion.2), channel_id=1, source_target_pairs={{0,1},{1,0},{2,3},{3,2},{4,5},{5,4},{6,7},{7,6},{8,9},{9,8},{10,11... | collective-permute-start | bytes 2359304 | tf_op jit(solution)/shard_map/ppermute | solution.py:502

commit v2 on v1

--- a/solution.py
+++ b/solution.py
@@ -18,7 +18,7 @@
 TOKEN_CHUNKS = 4
 
 
-def fused_plan(grp_count, sp_count, tp_count, rows, part, proj_rows, out_rows):
+def fused_plan(grp_count, sp_count, tp_count, rows, part, proj_rows, out_rows, q_width, k_width, c_width):
     lines = sp_count // 2
     return (
         grp_count == 2
@@ -28,22 +28,50 @@
         and proj_rows % (2 * PROJ_UNITS * 16) == 0
         and out_rows % (2 * OUT_UNITS * 16) == 0
         and rows % (TOKEN_CHUNKS * 16) == 0
-        and part % 128 == 0
-    )
-
-
-def gather_kernel(
+        and rows % (2 * WINDOW) == 0
+        and part % 256 == 0
+        and q_width % 256 == 0
+        and k_width == 128
+        and c_width % 256 == 0
+        and 2 * HEAD_DIM == 128
+    )
+
+
+def layer_kernel(
     sizes,
     tok_ref,
     gain_ref,
-    wp_ref,
-    wo_ref,
-    proj_ref,
+    wk_ref,
+    wv_ref,
+    wc_ref,
+    wu_ref,
+    wb_ref,
+    wq_ref,
+    wa_ref,
+    wm_ref,
+    sink_ref,
+    taps_ref,
+    bias_ref,
+    doc_ref,
+    doc_col,
+    cos_ref,
+    sin_ref,
+    out_ref,
+    wp_full,
     wo_full,
-    wp_full,
     tok_other,
     scaled,
     inv_ref,
+    proj_ref,
+    pair_ext,
+    query_s,
+    carried,
+    carry_near,
+    doc_row,
+    convolved,
+    conv_other,
+    attended,
+    att_other,
     z_send,
     z_recv,
     y_send,
@@ -57,12 +85,16 @@
     x_send,
     x_recv,
     own_sem,
+    halo_send,
+    halo_recv,
+    conv_sem,
+    att_send,
+    att_recv,
 ):
-    lines, cut = sizes
+    lines, rp, ro = sizes
     f32 = jnp.float32
     rows, part = tok_ref.shape
-    rp = wp_ref.shape[0]
-    ro = wo_ref.shape[0]
+    bf16 = jnp.bfloat16
     up, uo = rp // 2 // PROJ_UNITS, ro // 2 // OUT_UNITS
     y = lax.axis_index("grp")
     sp = lax.axis_index("sp")
@@ -89,13 +121,6 @@
         row = (zo * 2 + cc) * ro + h * (ro // 2) + (u - PROJ_UNITS) * uo
         return wo_full.at[pl.ds(pl.multiple_of(row, uo), uo), :]
 
-    def mine(u, h):
-        if u < PROJ_UNITS:
-            row = h * (rp // 2) + u * up
-            return wp_ref.at[pl.ds(pl.multiple_of(row, up), up), :]
-        row = h * (ro // 2) + (u - PROJ_UNITS) * uo
-        return wo_ref.at[pl.ds(pl.multiple_of(row, uo), uo), :]
-
     def remote(src, dst, send, recv, device):
         return pltpu.make_async_remote_copy(
             src_ref=src, dst_ref=dst, send_sem=send, recv_sem=recv,
@@ -105,8 +130,7 @@
     def z_copy(way, t, u):
         zo = origin(way, t)
         dst = place(u, zo, c, y)
-        src = mine(u, y) if t == 0 else dst
-        return remote(src, dst, z_send.at[way, t, u], z_recv.at[way, t, u], to_z[way])
+        return remote(dst, dst, z_send.at[way, t, u], z_recv.at[way, t, u], to_z[way])
 
     def z_arrival(way, t, u):
         dst = place(u, origin(way, t), c, y)
@@ -125,15 +149,28 @@
         ref = place(u, origin(way, t), cc, y if kind == 0 else 1 - y)
         return remote(ref, ref, send.at[way, t - 1, u], recv.at[way, t - 1, u], to_core)
 
+    def shard(group, cc):
+        full, size = (wp_full, rp) if group == 0 else (wo_full, ro)
+        return full, pl.ds(pl.multiple_of((z * 2 + cc) * size, size), size)
+
     def own_d(group, cc):
-        ref, full, size = (wp_ref, wp_full, rp) if group == 0 else (wo_ref, wo_full, ro)
-        dst = full.at[pl.ds(pl.multiple_of((z * 2 + cc) * size, size), size), :]
-        return remote(ref, dst, do_send.at[group], do_recv.at[group], to_core)
+        full, at = shard(group, cc)
+        dst = full.at[at, :]
+        return remote(dst, dst, do_send.at[group], do_recv.at[group], to_core)
 
     def own_local(group):
-        ref, full, size = (wp_ref, wp_full, rp) if group == 0 else (wo_ref, wo_full, ro)
-        dst = full.at[pl.ds(pl.multiple_of((z * 2 + c) * size, size), size), :]
-        return pltpu.make_async_copy(ref, dst, own_sem.at[group])
+        full, at = shard(group, c)
+        refs = (wk_ref, wv_ref, wc_ref, wu_ref, wb_ref, wq_ref) if group == 0 else (wa_ref, wm_ref)
+        copies, col = [], 0
+        for j, ref in enumerate(refs):
+            size = ref.shape[1]
+            copies.append(
+                pltpu.make_async_copy(
+                    ref, full.at[at, pl.ds(col, size)], own_sem.at[6 * group + j]
+                )
+            )
+            col += size
+        return copies
 
     chunk = rows // TOKEN_CHUNKS
 
@@ -143,6 +180,55 @@
             x_send.at[k], x_recv.at[k], to_x,
         )
 
+    last = 2 * lines - 1
+    steps_sp = (sp + 1, sp - 1)
+    sends_to = (sp < last, sp > 0)
+    gets_from = (sp > 0, sp < last)
+    side = jnp.where(c == 0, sp - 1, sp + 1)
+    has_side = (side >= 0) & (side <= last)
+
+    def halo(kind, way):
+        if kind == 0:
+            src = doc_ref.at[:, rows - WINDOW : rows] if way == 0 else doc_ref.at[:, 0:WINDOW]
+            at = 0 if way == 0 else WINDOW + rows
+            dst = doc_row.at[:, at : at + WINDOW]
+        elif kind == 1:
+            at = rows if way == 0 else WINDOW
+            src = pair_ext.at[at : at + WINDOW, :]
+            at = 0 if way == 0 else WINDOW + rows
+            dst = pair_ext.at[at : at + WINDOW, :]
+        else:
+            at = rows - 16 if way == 0 else 0
+            src = carried.at[at : at + 16, :]
+            dst = carry_near.at[way]
+        return remote(
+            src, dst, halo_send.at[kind, way], halo_recv.at[kind, way], {"sp": steps_sp[way]}
+        )
+
+    def start_halo(kind):
+        for way in range(2):
+
+            @pl.when(sends_to[way])
+            def _():
+                halo(kind, way).start()
+
+    def wait_halo(kind):
+        for way in range(2):
+
+            @pl.when(gets_from[way])
+            def _():
+                halo(kind, way).wait_recv()
+
+    def conv_copy():
+        return remote(convolved, conv_other, conv_sem.at[0], conv_sem.at[1], to_x)
+
+    def att_copy(i):
+        at = pl.ds(pl.multiple_of(i * WINDOW, WINDOW), WINDOW)
+        return remote(attended.at[at, :], att_other.at[at, :], att_send.at[i], att_recv.at[i], to_x)
+
+    for copy in own_local(0) + own_local(1):
+        copy.start()
+
     barrier = pltpu.get_barrier_semaphore()
     for device in (to_y, to_core, to_x):
         pl.semaphore_signal(barrier, inc=1, device_id=device, device_id_type=pl.DeviceIdType.MESH)
@@ -154,7 +240,13 @@
                 barrier, inc=1, device_id=to_z[way], device_id_type=pl.DeviceIdType.MESH
             )
 
-    neighbours = jnp.where(z > 0, 1, 0) + jnp.where(z < lines - 1, 1, 0) + 3
+    @pl.when(has_side)
+    def _():
+        pl.semaphore_signal(
+            barrier, inc=1, device_id={"sp": side}, device_id_type=pl.DeviceIdType.MESH
+        )
+
+    neighbours = jnp.where(has_side, 1, 0) + jnp.where(z > 0, 1, 0) + jnp.where(z < lines - 1, 1, 0) + 3
     pl.semaphore_wait(barrier, neighbours)
 
     def start_own(units):
@@ -165,11 +257,25 @@
                 def _():
                     z_copy(way, 0, u).start()
 
-    start_own(proj_units)
     for k in range(TOKEN_CHUNKS):
         x_copy(k).start()
+    for copy in own_local(0):
+        copy.wait()
+    start_own(proj_units)
     own_d(0, c).start()
-    own_local(0).start()
+    start_halo(0)
+    doc_row[:, WINDOW : WINDOW + rows] = doc_ref[...]
+
+    @pl.when(sp == 0)
+    def _():
+        doc_row[:, :WINDOW] = jnp.full((doc_row.shape[0], WINDOW), -1.0, f32)
+        pair_ext[:WINDOW, :] = jnp.zeros((WINDOW, pair_ext.shape[1]), bf16)
+
+    @pl.when(sp == last)
+    def _():
+        doc_row[:, WINDOW + rows :] = jnp.full((doc_row.shape[0], WINDOW), -1.0, f32)
+        pair_ext[WINDOW + rows :, :] = jnp.zeros((WINDOW, pair_ext.shape[1]), bf16)
+
 
     def event(t, u):
         for way in range(2):
@@ -227,9 +333,10 @@
         if i >= 1:
             y_event(*steps[i - 1])
         if (t, u) == (lines - 1, 0):
+            for copy in own_local(1):
+                copy.wait()
             start_own(out_units)
             own_d(1, c).start()
-            own_local(1).start()
         while done < TOKEN_CHUNKS - 1 and (i + 1) * TOKEN_CHUNKS >= (done + 1) * len(steps):
             scale(done)
             done += 1
@@ -238,7 +345,6 @@
         scale(done)
         done += 1
     own_d(0, 1 - c).wait_recv()
-    own_local(0).wait()
     for t, u in steps:
         for way in range(2):
 
@@ -247,10 +353,22 @@
                 d_copy(0, way, t, u, 1 - c).wait_recv()
                 d_copy(1, way, t, u, 1 - c).wait_recv()
 
-    width = proj_ref.shape[1]
-    blocks = width // cut
     tail = [(t, u) for t in range(1, lines) for u in out_units]
-    cuts = [blocks * i // len(tail) for i in range(len(tail) + 1)]
+    pending = list(enumerate(tail))
+    beats = 6
+
+    def advance(beat):
+        goal = len(tail) * (beats - 1 - beat) // beats
+        while len(pending) > goal:
+            i, (t, u) = pending.pop(0)
+            event(t, u)
+            if i >= 1:
+                y_event(*tail[i - 1])
+
+    cut = 256
+    k_width, c_width, q_width = wk_ref.shape[1], wc_ref.shape[1], wq_ref.shape[1]
+    c_at = 2 * k_width
+    u_at, b_at, q_at = c_at + c_width, c_at + 2 * c_width, c_at + 3 * c_width
 
     def project(begin, end):
         def body(j, carry):
@@ -259,16 +377,133 @@
             proj_ref[:, at] = acc * inv_ref[:, :1]
             return carry
 
-        lax.fori_loop(begin, end, body, 0)
-
-    for i, (t, u) in enumerate(tail):
-        project(cuts[i], cuts[i + 1])
-        event(t, u)
-        if i >= 1:
-            y_event(*tail[i - 1])
+        lax.fori_loop(begin // cut, end // cut, body, 0)
+
+    lanes = 128
+    lane = lax.broadcasted_iota(jnp.int32, (rows, lanes), 1)
+    low = (lane % HEAD_DIM) < HEAD_DIM // 2
+
+    def turned(cells):
+        ahead = pltpu.roll(cells, lanes - HEAD_DIM // 2, 1)
+        behind = pltpu.roll(cells, HEAD_DIM // 2, 1)
+        return cells * cos_ref[...] + jnp.where(low, ahead, behind) * sin_ref[...]
+
+    def block(at, j):
+        return pl.ds(pl.multiple_of(at + j * lanes, lanes), lanes)
+
+    project(0, c_at)
+    pair_ext[WINDOW : WINDOW + rows, :k_width] = turned(proj_ref[:, :k_width]).astype(bf16)
+    pair_ext[WINDOW : WINDOW + rows, k_width:] = proj_ref[:, k_width : 2 * k_width].astype(bf16)
+    advance(0)
+    start_halo(1)
+    project(c_at, b_at)
+
+    def carry_body(j, carry):
+        carried[:, block(0, j)] = (
+            proj_ref[:, block(c_at, j)] * proj_ref[:, block(u_at, j)]
+        ).astype(bf16)
+        return carry
+
+    lax.fori_loop(0, c_width // lanes, carry_body, 0)
+    advance(1)
+    start_halo(2)
+    project(b_at, q_at)
+    advance(2)
+    wait_halo(0)
+    wait_halo(2)
+
+    row = lax.broadcasted_iota(jnp.int32, (rows, lanes), 0)
+
+    def conv_body(j, carry):
+        at = block(0, j)
+        docs = doc_col[...]
+        cells = carried[:, at].astype(f32)
+        before = jnp.where(row == 0, carry_near[0, 15:16, at].astype(f32), pltpu.roll(cells, 1, 0))
+        after = jnp.where(
+            row == rows - 1, carry_near[1, 0:1, at].astype(f32), pltpu.roll(cells, rows - 1, 0)
+        )
+        doc_before = jnp.where(row == 0, doc_row[0:1, WINDOW - 1 : WINDOW], pltpu.roll(docs, 1, 0))
+        doc_after = jnp.where(
+            row == rows - 1,
+            doc_row[0:1, WINDOW + rows : WINDOW + rows + 1],
+            pltpu.roll(docs, rows - 1, 0),
+        )
+        conv = jnp.where(doc_before == docs, before * taps_ref[0:1, at], 0.0)
+        conv = conv + cells * taps_ref[1:2, at]
+        conv = conv + jnp.where(doc_after == docs, after * taps_ref[2:3, at], 0.0)
+        convolved[:, at] = (proj_ref[:, block(b_at, j)] * (conv + bias_ref[:, at])).astype(bf16)
+        return carry
+
+    lax.fori_loop(0, c_width // lanes, conv_body, 0)
+    project(q_at, q_at + q_width)
+    conv_copy().start()
+    advance(3)
+
+    def query_body(j, carry):
+        cells = turned(proj_ref[:, block(q_at, j)])
+        query_s[:, block(0, j)] = (cells * HEAD_DIM ** (-0.5)).astype(bf16)
+        return carry
+
+    lax.fori_loop(0, q_width // lanes, query_body, 0)
+    wait_halo(1)
+    kv_heads = k_width // HEAD_DIM
+    groups = q_width // HEAD_DIM // kv_heads
+    span = 3 * WINDOW
+    gap = lax.broadcasted_iota(jnp.int32, (WINDOW, span), 1) - lax.broadcasted_iota(
+        jnp.int32, (WINDOW, span), 0
+    )
+    window = (gap >= 0) & (gap <= 2 * WINDOW)
+
+    def attend(i, carry):
+        at = pl.ds(pl.multiple_of(i * WINDOW, WINDOW), WINDOW)
+        near = pl.ds(pl.multiple_of(i * WINDOW, WINDOW), span)
+        allowed = window & (doc_col[at, 0:1] == doc_row[0:1, near])
+        bias = jnp.where(allowed, 0.0, -jnp.inf)
+        bias = jnp.concatenate([bias] * groups, axis=0)
+        queries = query_s[at, :]
+        pairs = pair_ext[near, :]
+        for head in range(kv_heads):
+            keys = pairs[:, head * HEAD_DIM : (head + 1) * HEAD_DIM]
+            values = pairs[:, k_width + head * HEAD_DIM : k_width + (head + 1) * HEAD_DIM]
+            first = head * groups
+            stack = jnp.concatenate(
+                [
+                    queries[:, (first + g) * HEAD_DIM : (first + g + 1) * HEAD_DIM]
+                    for g in range(groups)
+                ],
+                axis=0,
+            )
+            sinks = jnp.concatenate(
+                [jnp.full((WINDOW, 1), sink_ref[first + g], f32) for g in range(groups)], axis=0
+            )
+            scores = lax.dot_general(
+                stack, keys, (((1,), (1,)), ((), ())), preferred_element_type=f32
+            )
+            scores = scores + bias
+            top = jnp.maximum(jnp.max(scores, axis=1, keepdims=True), sinks)
+            expo = jnp.exp(scores - top)
+            total = jnp.sum(expo, axis=1, keepdims=True) + jnp.exp(sinks - top)
+            weight = (expo * (1.0 / total)).astype(bf16)
+            result = jnp.dot(weight, values, preferred_element_type=f32).astype(bf16)
+            wide = jnp.concatenate(
+                [result[g * WINDOW : (g + 1) * WINDOW] for g in range(groups)], axis=1
+            )
+            attended[at, first * HEAD_DIM : (first + groups) * HEAD_DIM] = wide
+
+        @pl.when(i > 0)
+        def _():
+            att_copy(i - 1).start()
+
+        return carry
+
+    blocks = rows // WINDOW
+    lax.fori_loop(0, blocks // 2, attend, 0)
+    advance(4)
+    lax.fori_loop(blocks // 2, blocks, attend, 0)
+    advance(5)
+    att_copy(blocks - 1).start()
     y_event(*tail[-1])
     own_d(1, 1 - c).wait_recv()
-    own_local(1).wait()
     for t, u in tail:
         for way in range(2):
 
@@ -277,6 +512,49 @@
                 d_copy(0, way, t, u, 1 - c).wait_recv()
                 d_copy(1, way, t, u, 1 - c).wait_recv()
 
+    conv_copy().wait_recv()
+    q_mine = pl.ds(pl.multiple_of(x * q_width, q_width), q_width)
+    q_yours = pl.ds(pl.multiple_of((1 - x) * q_width, q_width), q_width)
+    c_mine = pl.ds(pl.multiple_of(x * c_width, c_width), c_width)
+    c_yours = pl.ds(pl.multiple_of((1 - x) * c_width, c_width), c_width)
+
+    def mix_body(j, carry):
+        at = pl.ds(pl.multiple_of(j * cut, cut), cut)
+        late = pl.ds(pl.multiple_of(part + j * cut, cut), cut)
+        acc = jnp.dot(attended[...], wo_full[q_mine, at], preferred_element_type=f32)
+        acc = acc + jnp.dot(convolved[...], wo_full[c_mine, late], preferred_element_type=f32)
+        acc = acc + jnp.dot(conv_other[...], wo_full[c_yours, late], preferred_element_type=f32)
+        proj_ref[:, at] = acc
+        return carry
+
+    lax.fori_loop(0, part // cut, mix_body, 0)
+    half = rows // 2
+    for k in range(2):
+        for i in range(k * blocks // 2, (k + 1) * blocks // 2):
+            att_copy(i).wait_recv()
+
+        def last_body(j, carry):
+            at = pl.ds(pl.multiple_of(j * cut, cut), cut)
+            acc = proj_ref[k * half : (k + 1) * half, at] + jnp.dot(
+                att_other[k * half : (k + 1) * half, :],
+                wo_full[q_yours, at],
+                preferred_element_type=f32,
+            )
+            out_ref[k * half : (k + 1) * half, at] = acc.astype(bf16)
+            return carry
+
+        lax.fori_loop(0, part // cut, last_body, 0)
+
+    for kind in range(3):
+        for way in range(2):
+
+            @pl.when(sends_to[way])
+            def _():
+                halo(kind, way).wait_send()
+
+    conv_copy().wait_send()
+    for i in range(blocks):
+        att_copy(i).wait_send()
     for group in range(2):
         own_d(group, c).wait_send()
     for k in range(TOKEN_CHUNKS):
@@ -303,38 +581,78 @@
                     d_copy(1, way, t, u, c).wait_send()
 
 
-def gather_project(tokens, gain, w_proj, w_out, sp_count):
+def fused_layer(
+    tokens, gain, projections, outputs, sink_logit, taps, conv_bias, documents, sp_count
+):
     rows, part = tokens.shape
+    f32 = jnp.float32
+    bf16 = jnp.bfloat16
     lines = sp_count // 2
-    width = w_proj.shape[1]
-    cut = 256 if width % 256 == 0 else 128
-    units = PROJ_UNITS + OUT_UNITS
+    wk, wv, wc, wu, wb, wq = projections
+    width = sum(w.shape[1] for w in projections)
+    rp, ro = wq.shape[0], outputs[0].shape[0]
+    q_width, k_width, c_width = wq.shape[1], wk.shape[1], wc.shape[1]
+    half = HEAD_DIM // 2
+    lanes = 128
+    positions = lax.axis_index("sp") * rows + jnp.arange(rows, dtype=jnp.int32)
+    freq = jnp.power(THETA, -(jnp.arange(half, dtype=f32) * (2.0 / HEAD_DIM)))
+    angle = positions.astype(f32)[:, None] * freq[None, :]
+    cosine, sine = jnp.cos(angle), jnp.sin(angle)
+    cosine = jnp.concatenate([cosine] * (lanes // half), axis=1)
+    sine = jnp.concatenate([-sine, sine] * (lanes // HEAD_DIM), axis=1)
+    docs = documents.astype(f32)
+    doc_rows = jnp.broadcast_to(docs[None, :], (8, rows))
+    doc_cols = jnp.broadcast_to(docs[:, None], (rows, lanes))
+    blocks = rows // WINDOW
     dma = pltpu.SemaphoreType.DMA
-    hops = (2, lines - 1, units)
+    hops = (2, lines - 1, PROJ_UNITS + OUT_UNITS)
     vmem = pl.BlockSpec(memory_space=pltpu.VMEM)
+    hbm = pl.BlockSpec(memory_space=pl.ANY)
+    smem = pl.BlockSpec(memory_space=pltpu.SMEM)
     flops = 2 * rows * 2 * part * width
     return pl.pallas_call(
-        functools.partial(gather_kernel, (lines, cut)),
-        out_shape=(
-            jax.ShapeDtypeStruct((rows, width), jnp.float32),
-            jax.ShapeDtypeStruct((w_out.shape[0] * sp_count, w_out.shape[1]), w_out.dtype),
-        ),
-        in_specs=[vmem] * 4,
-        out_specs=(vmem, pl.BlockSpec(memory_space=pl.ANY)),
+        functools.partial(layer_kernel, (lines, rp, ro)),
+        out_shape=jax.ShapeDtypeStruct((rows, part), bf16),
+        in_specs=[vmem] * 2 + [hbm] * 8 + [smem] + [vmem] * 6,
+        out_specs=vmem,
         scratch_shapes=[
-            pltpu.VMEM((w_proj.shape[0] * sp_count, width), w_proj.dtype),
-            pltpu.VMEM((rows, part), tokens.dtype),
-            pltpu.VMEM((rows, 2 * part), jnp.bfloat16),
-            pltpu.VMEM((rows, 128), jnp.float32),
+            pltpu.VMEM((rp * sp_count, width), bf16),
+            pltpu.VMEM((ro * sp_count, 2 * part), bf16),
+            pltpu.VMEM((rows, part), bf16),
+            pltpu.VMEM((rows, 2 * part), bf16),
+            pltpu.VMEM((rows, 128), f32),
+            pltpu.VMEM((rows, max(width, part)), f32),
+            pltpu.VMEM((rows + 2 * WINDOW, 2 * k_width), bf16),
+            pltpu.VMEM((rows, q_width), bf16),
+            pltpu.VMEM((rows, c_width), bf16),
+            pltpu.VMEM((2, 16, c_width), bf16),
+            pltpu.VMEM((8, rows + 2 * WINDOW), f32),
+            pltpu.VMEM((rows, c_width), bf16),
+            pltpu.VMEM((rows, c_width), bf16),
+            pltpu.VMEM((rows, q_width), bf16),
+            pltpu.VMEM((rows, q_width), bf16),
         ]
         + [dma(hops)] * 8
-        + [dma((2,)), dma((2,)), dma((TOKEN_CHUNKS,)), dma((TOKEN_CHUNKS,)), dma((2,))],
+        + [dma((2,)), dma((2,)), dma((TOKEN_CHUNKS,)), dma((TOKEN_CHUNKS,)), dma((8,))]
+        + [dma((3, 2)), dma((3, 2)), dma((2,)), dma((blocks,)), dma((blocks,))],
         compiler_params=pltpu.CompilerParams(
-            collective_id=0, has_side_effects=True, vmem_limit_bytes=60 * 1024 * 1024
+            collective_id=0, has_side_effects=True, vmem_limit_bytes=62 * 1024 * 1024
         ),
         cost_estimate=pl.CostEstimate(flops=flops, bytes_accessed=0, transcendentals=0),
-        name="gather_project",
-    )(tokens, gain[None, :], w_proj, w_out)
+        name="layer",
+    )(
+        tokens,
+        gain[None, :],
+        *projections,
+        *outputs,
+        sink_logit,
+        taps,
+        conv_bias[None, :],
+        doc_rows,
+        doc_cols,
+        cosine,
+        sine,
+    )
 
 
 def extended(cells, sides, width):
@@ -405,44 +723,47 @@
     kv_local = w_key.shape[1] // head_dim
     groups = q_local // kv_local
     if fused_plan(
-        lax.axis_size("grp"), sp_count, tp_count, rows, part, w_query.shape[0], w_attn_out.shape[0]
+        lax.axis_size("grp"),
+        sp_count,
+        tp_count,
+        rows,
+        part,
+        w_query.shape[0],
+        w_attn_out.shape[0],
+        w_query.shape[1],
+        w_key.shape[1],
+        w_input.shape[1],
     ):
-        cols = (w_query, w_key, w_value, w_input, w_bgate, w_cgate)
-        proj, w_both = gather_project(
+        return fused_layer(
             tokens,
             gain,
-            jnp.concatenate(cols, axis=1),
-            jnp.concatenate((w_attn_out, w_conv_out), axis=1),
+            (w_key, w_value, w_cgate, w_input, w_bgate, w_query),
+            (w_attn_out, w_conv_out),
+            sink_logit,
+            taps,
+            conv_bias,
+            documents,
             sp_count,
         )
-        parts, at = [], 0
-        for col in cols:
-            parts.append(proj[:, at : at + col.shape[1]])
-            at += col.shape[1]
-        q_acc, k_acc, v_acc, u_acc, b_acc, c_acc = parts
-        w_attn = w_both[:, :part]
-        w_conv = w_both[:, part:]
-        inv = jnp.float32(1.0)
-    else:
-        wq, wk, wv, wu, wb, wc, w_attn, w_conv = (
-            lax.all_gather(w_query, "sp", axis=0, tiled=True),
-            lax.all_gather(w_key, "sp", axis=0, tiled=True),
-            lax.all_gather(w_value, "sp", axis=0, tiled=True),
-            lax.all_gather(w_input, "sp", axis=0, tiled=True),
-            lax.all_gather(w_bgate, "sp", axis=0, tiled=True),
-            lax.all_gather(w_cgate, "sp", axis=0, tiled=True),
-            lax.all_gather(w_attn_out, "sp", axis=0, tiled=True),
-            lax.all_gather(w_conv_out, "sp", axis=0, tiled=True),
-        )
-        matrices = (wq, wk, wv, wu, wb, wc)
-        piece_f = lax.all_gather(tokens, "tp", axis=1, tiled=True).astype(f32)
-        scaled = (piece_f * gain[None, :]).astype(bf16)
-        products = tuple((jnp.dot(scaled, mat, preferred_element_type=f32) for mat in matrices))
-        folded = products + (jnp.sum(piece_f * piece_f, axis=1),)
-        sums = folded[:6]
-        squares = folded[6]
-        inv = lax.rsqrt(squares / width + EPS)[:, None]
-        q_acc, k_acc, v_acc, u_acc, b_acc, c_acc = sums
+    wq, wk, wv, wu, wb, wc, w_attn, w_conv = (
+        lax.all_gather(w_query, "sp", axis=0, tiled=True),
+        lax.all_gather(w_key, "sp", axis=0, tiled=True),
+        lax.all_gather(w_value, "sp", axis=0, tiled=True),
+        lax.all_gather(w_input, "sp", axis=0, tiled=True),
+        lax.all_gather(w_bgate, "sp", axis=0, tiled=True),
+        lax.all_gather(w_cgate, "sp", axis=0, tiled=True),
+        lax.all_gather(w_attn_out, "sp", axis=0, tiled=True),
+        lax.all_gather(w_conv_out, "sp", axis=0, tiled=True),
+    )
+    matrices = (wq, wk, wv, wu, wb, wc)
+    piece_f = lax.all_gather(tokens, "tp", axis=1, tiled=True).astype(f32)
+    scaled = (piece_f * gain[None, :]).astype(bf16)
+    products = tuple((jnp.dot(scaled, mat, preferred_element_type=f32) for mat in matrices))
+    folded = products + (jnp.sum(piece_f * piece_f, axis=1),)
+    sums = folded[:6]
+    squares = folded[6]
+    inv = lax.rsqrt(squares / width + EPS)[:, None]
+    q_acc, k_acc, v_acc, u_acc, b_acc, c_acc = sums
     positions = lax.axis_index("sp") * rows + jnp.arange(rows, dtype=jnp.int32)
     query = rotate(q_acc * inv, positions, q_local).astype(bf16)
     keys = rotate(k_acc * inv, positions, kv_local).astype(bf16)
@@ -493,22 +814,12 @@
             same, carry_ext[tap : tap + rows].astype(f32) * taps[tap][None, :], 0.0
         )
     convolved = (bgate * (conv + conv_bias[None, :])).astype(bf16)
-    me = lax.axis_index("tp")
-    terms = []
-    for shift in range(tp_count):
-        hops = [(i, (i + shift) % tp_count) for i in range(tp_count)]
-        owner = (me + tp_count - shift) % tp_count
-        for mixer, weight in ((convolved, w_conv), (attended, w_attn)):
-            piece = mixer if shift == 0 else lax.ppermute(mixer, "tp", hops)
-            span = piece.shape[1]
-            terms.append(
-                jnp.dot(
-                    piece,
-                    lax.dynamic_slice_in_dim(weight, owner * span, span, 0),
-                    preferred_element_type=f32,
-                )
-            )
-    mixed = functools.reduce(jnp.add, terms)
+    acc = jnp.dot(
+        lax.all_gather(attended, "tp", axis=1, tiled=True), w_attn, preferred_element_type=f32
+    )
+    mixed = acc + jnp.dot(
+        lax.all_gather(convolved, "tp", axis=1, tiled=True), w_conv, preferred_element_type=f32
+    )
     return mixed.astype(bf16)
 
 

time: 194 us -> 120 us (0.62)
  Pallas kernels: 86.2 us -> 111 us
  local copies, waits for them, and re-layouts: 26 us -> 4.18 us
  matrix products: 21.5 us -> 0 us
  starting transfers between devices: 21.4 us -> 0 us
  other arithmetic: 23.2 us -> 3.73 us
  waiting for transfers between devices: 14 us -> 0 us
    pallas_call x1, Pallas kernels: 86.2 us -> 111 us  [fused_layer(): pl.pallas_call(functools.partial(layer_kernel, (lines, rp, ro)), out_shap...]
    dot_general x8 -> x0, matrix products: 21.5 us -> none  [the longest x2 11.2 us: local(): jnp.einsum('hgqk,khd->qhgd', weight, v_block, preferred_element_type=f32)]
    ppermute x10 -> x0, starting transfers between devices: 21.4 us -> none  [the longest x4 14 us: extended(): lax.ppermute(tail, axis, [(i, (i + 1) % count) for i in range(ends)])]
    slice x18 -> x0, local copies, waits for them, and re-layouts: 16.4 us -> none  [the longest x4 5.41 us: local(): parts.append(proj[:, at:at + col.shape[1]])]
    ppermute x10 -> x0, waiting for transfers between devices: 14 us -> none  [the longest x2 14 us: local(): piece = mixer if shift == 0 else lax.ppermute(mixer, 'tp', hops)]
    unnamed x45 -> x1, local copies, waits for them, and re-layouts: 7.77 us -> 2.67 us
    slice x2 -> x0, other arithmetic: 4.57 us -> none  [the longest x1 3.87 us: local(): parts.append(proj[:, at:at + col.shape[1]])]
    convert_element_type x4 -> x2, other arithmetic: 4.65 us -> 0.7 us  [the longest x1 0.69 us: fused_layer(): docs = documents.astype(f32)]
  transfers between devices with their start and end apart: 10 -> 0, of which waited for: 1 -> 0; matrix products, arithmetic and copies ran while one was open for 28% -> 0% of each run, Pallas kernels for 0% -> 0%
where the time goes in v2:
time: 120 us; the launch traced here: 119 us
  Pallas kernels  111 us (92%)
  local copies, waits for them, and re-layouts  4.18 us (3%)
  other arithmetic  3.73 us (3%)
    pallas_call x1, Pallas kernels, fused_layer(): pl.pallas_call(functools.partial(layer_kernel, (lines, rp, ro)), out_shap...  111 us
    unnamed x1, local copies, waits for them, and re-layouts  2.67 us

profile of v2, /device:TPU:0, one launch (start us, length us, event | category | flops | bytes accessed | tf_op | source)
XLA Modules:
  0.0 119.4 jit_solution(4984100042405205452)
XLA Ops:
  0.0 0.7 convert_element_type.10
  0.7 0.6 broadcast_in_dim.10.doc_ref
  1.3 0.9 broadcast_in_dim.11.doc_col
  2.2 1.4 %fusion = (f32[768,32]{1,0:T(8,128)S(1)}, f32[768,32]{1,0:T(8,128)S(1)}, f32[768,32]{1,0:T(8,128)S(1)}) fusion(f32[32]{0:T(128)S(1)} %negate_power_fusion, f32[768]{0:T(1024)S(1)} %add_convert_fusion), kind=kLoop, calls=%fused_computation.4 | loop fusion | flops 49152 | bytes 298112 | tf_op jit(solution)/shard_map/neg | solution.py:602
  3.7 1.6 %pad_maximum_fusion = (f32[768,128]{1,0:T(8,128)}, f32[768,128]{1,0:T(8,128)}) fusion(f32[768,32]{1,0:T(8,128)S(1)} %get-tuple-element.7, f32[768,32]{1,0:T(8,128)S(1)} %get-tuple-element.6, f32[768,32]{1,0:T(8,128)S(1)} %get-tuple-element.5), kind=kLoop, calls=%fused_computation.2 | loop fusion | flops 589824 | bytes 1081344 | tf_op jit(solution)/shard_map/concatenate | solution.py:601
  5.3 111.4 %layer.1 = bf16[768,1024]{1,0:T(8,128)(2,1)} custom-call(bf16[768,1024]{1,0:T(8,128)(2,1)} %tok_ref.1, f32[1,2048]{1,0:T(1,128)} %bitcast.2, bf16[256,128]{1,0:T(8,128)(2,1)} %wk_ref.1, bf16[256,128]{1,0:T(8,128)(2,1)} %wv_ref.1, bf16[256,512]{1,0:T(8,128)(2,1)} %wc_ref.1, bf16[256,512]{1,0:T(8,128)(2,1)} %wu_ref.1, bf16[256,512]{1,0:T(8,128)(2,1)} %wb_ref.1, ...), custom_call_target="tpu_custom_call" | custom-call | flops 7247757312 | tf_op jit(solution)/shard_map/layer/pallas_call | solution.py:613
  116.7 2.7 %copy.17 = bf16[768,1024]{1,0:T(8,128)(2,1)} copy(bf16[768,1024]{1,0:T(8,128)(2,1)} %layer.1) | data formatting | bytes 3145728
  (2 shorter events, 0.0 us)

commit v3 on v2

--- a/solution.py
+++ b/solution.py
@@ -13,8 +13,10 @@
 
 EPS = 1e-06
 THETA = 500000.0
-PROJ_UNITS = 4
+CONV_UNITS = 4
+ATT_UNITS = 2
 OUT_UNITS = 2
+LATE = 3
 TOKEN_CHUNKS = 4
 
 
@@ -25,7 +27,8 @@
         and tp_count == 2
         and sp_count % 2 == 0
         and 2 <= lines <= 4
-        and proj_rows % (2 * PROJ_UNITS * 16) == 0
+        and proj_rows % (2 * CONV_UNITS * 16) == 0
+        and proj_rows % (2 * ATT_UNITS * 16) == 0
         and out_rows % (2 * OUT_UNITS * 16) == 0
         and rows % (TOKEN_CHUNKS * 16) == 0
         and rows % (2 * WINDOW) == 0
@@ -95,13 +98,23 @@
     f32 = jnp.float32
     rows, part = tok_ref.shape
     bf16 = jnp.bfloat16
-    up, uo = rp // 2 // PROJ_UNITS, ro // 2 // OUT_UNITS
+    k_width, c_width, q_width = wk_ref.shape[1], wc_ref.shape[1], wq_ref.shape[1]
+    k_at = 3 * c_width
+    q_at = k_at + 2 * k_width
+    width = q_at + q_width
     y = lax.axis_index("grp")
     sp = lax.axis_index("sp")
     x = lax.axis_index("tp")
     z, c = sp // 2, sp % 2
-    proj_units = list(range(PROJ_UNITS))
-    out_units = list(range(PROJ_UNITS, PROJ_UNITS + OUT_UNITS))
+    groups_of = []
+    for full, size, count, cols in (
+        (wp_full, rp, CONV_UNITS, (0, k_at)),
+        (wp_full, rp, ATT_UNITS, (k_at, width)),
+        (wo_full, ro, OUT_UNITS, (0, 2 * part)),
+    ):
+        groups_of += [(full, size, size // 2 // count, j, cols) for j in range(count)]
+    ends = (CONV_UNITS, CONV_UNITS + ATT_UNITS, CONV_UNITS + ATT_UNITS + OUT_UNITS)
+    units_of = (range(0, ends[0]), range(ends[0], ends[1]), range(ends[1], ends[2]))
     to_y = {"grp": 1 - y}
     to_core = {"sp": z * 2 + 1 - c}
     to_x = {"tp": 1 - x}
@@ -115,11 +128,9 @@
         return z >= t if way == 0 else z < lines - t
 
     def place(u, zo, cc, h):
-        if u < PROJ_UNITS:
-            row = (zo * 2 + cc) * rp + h * (rp // 2) + u * up
-            return wp_full.at[pl.ds(pl.multiple_of(row, up), up), :]
-        row = (zo * 2 + cc) * ro + h * (ro // 2) + (u - PROJ_UNITS) * uo
-        return wo_full.at[pl.ds(pl.multiple_of(row, uo), uo), :]
+        full, size, tall, j, cols = groups_of[u]
+        row = (zo * 2 + cc) * size + h * (size // 2) + j * tall
+        return full.at[pl.ds(pl.multiple_of(row, tall), tall), cols[0] : cols[1]]
 
     def remote(src, dst, send, recv, device):
         return pltpu.make_async_remote_copy(
@@ -150,23 +161,24 @@
         return remote(ref, ref, send.at[way, t - 1, u], recv.at[way, t - 1, u], to_core)
 
     def shard(group, cc):
-        full, size = (wp_full, rp) if group == 0 else (wo_full, ro)
-        return full, pl.ds(pl.multiple_of((z * 2 + cc) * size, size), size)
+        full, size, _, _, cols = groups_of[ends[group] - 1]
+        return full, pl.ds(pl.multiple_of((z * 2 + cc) * size, size), size), cols
 
     def own_d(group, cc):
-        full, at = shard(group, cc)
-        dst = full.at[at, :]
+        full, at, cols = shard(group, cc)
+        dst = full.at[at, cols[0] : cols[1]]
         return remote(dst, dst, do_send.at[group], do_recv.at[group], to_core)
 
+    own_refs = ((wc_ref, wu_ref, wb_ref), (wk_ref, wv_ref, wq_ref), (wa_ref, wm_ref))
+
     def own_local(group):
-        full, at = shard(group, c)
-        refs = (wk_ref, wv_ref, wc_ref, wu_ref, wb_ref, wq_ref) if group == 0 else (wa_ref, wm_ref)
-        copies, col = [], 0
-        for j, ref in enumerate(refs):
+        full, at, cols = shard(group, c)
+        copies, col = [], cols[0]
+        for j, ref in enumerate(own_refs[group]):
             size = ref.shape[1]
             copies.append(
                 pltpu.make_async_copy(
-                    ref, full.at[at, pl.ds(col, size)], own_sem.at[6 * group + j]
+                    ref, full.at[at, col : col + size], own_sem.at[3 * group + j]
                 )
             )
             col += size
@@ -226,7 +238,7 @@
         at = pl.ds(pl.multiple_of(i * WINDOW, WINDOW), WINDOW)
         return remote(attended.at[at, :], att_other.at[at, :], att_send.at[i], att_recv.at[i], to_x)
 
-    for copy in own_local(0) + own_local(1):
+    for copy in own_local(0) + own_local(1) + own_local(2):
         copy.start()
 
     barrier = pltpu.get_barrier_semaphore()
@@ -261,7 +273,7 @@
         x_copy(k).start()
     for copy in own_local(0):
         copy.wait()
-    start_own(proj_units)
+    start_own(units_of[0])
     own_d(0, c).start()
     start_halo(0)
     doc_row[:, WINDOW : WINDOW + rows] = doc_ref[...]
@@ -326,49 +338,51 @@
 
         lax.fori_loop(0, chunk // tile, body, 0)
 
-    steps = [(t, u) for t in range(1, lines) for u in proj_units]
-    done = 0
-    for i, (t, u) in enumerate(steps):
-        event(t, u)
-        if i >= 1:
-            y_event(*steps[i - 1])
-        if (t, u) == (lines - 1, 0):
-            for copy in own_local(1):
-                copy.wait()
-            start_own(out_units)
-            own_d(1, c).start()
-        while done < TOKEN_CHUNKS - 1 and (i + 1) * TOKEN_CHUNKS >= (done + 1) * len(steps):
-            scale(done)
-            done += 1
-    y_event(*steps[-1])
-    while done < TOKEN_CHUNKS:
-        scale(done)
-        done += 1
-    own_d(0, 1 - c).wait_recv()
-    for t, u in steps:
-        for way in range(2):
-
-            @pl.when(arrives(way, t))
-            def _():
-                d_copy(0, way, t, u, 1 - c).wait_recv()
-                d_copy(1, way, t, u, 1 - c).wait_recv()
-
-    tail = [(t, u) for t in range(1, lines) for u in out_units]
-    pending = list(enumerate(tail))
-    beats = 6
-
-    def advance(beat):
-        goal = len(tail) * (beats - 1 - beat) // beats
-        while len(pending) > goal:
-            i, (t, u) = pending.pop(0)
-            event(t, u)
-            if i >= 1:
-                y_event(*tail[i - 1])
+    queue, marks = [], []
+    for units in units_of:
+        queue += [(t, u) for t in range(1, lines) for u in units]
+        marks.append(len(queue))
+    openers = {marks[g] - len(units_of[g]): g + 1 for g in range(2)}
+    state = [0, 0]
+
+    def advance(goal):
+        while state[0] < goal:
+            i = state[0]
+            event(*queue[i])
+            if i in openers:
+                group = openers[i]
+                for copy in own_local(group):
+                    copy.wait()
+                start_own(units_of[group])
+                own_d(group, c).start()
+            state[0] += 1
+            while state[1] < state[0] - LATE:
+                y_event(*queue[state[1]])
+                state[1] += 1
+
+    def settle(group):
+        advance(marks[group])
+        while state[1] < marks[group]:
+            y_event(*queue[state[1]])
+            state[1] += 1
+        own_d(group, 1 - c).wait_recv()
+        for t, u in queue[marks[group - 1] if group else 0 : marks[group]]:
+            for way in range(2):
+
+                @pl.when(arrives(way, t))
+                def _():
+                    d_copy(0, way, t, u, 1 - c).wait_recv()
+                    d_copy(1, way, t, u, 1 - c).wait_recv()
+
+    for k in range(TOKEN_CHUNKS - 1):
+        advance(marks[0] * (k + 1) // (TOKEN_CHUNKS - 1))
+        scale(k)
+    advance(marks[0] + 2)
+    settle(0)
+    scale(TOKEN_CHUNKS - 1)
 
     cut = 256
-    k_width, c_width, q_width = wk_ref.shape[1], wc_ref.shape[1], wq_ref.shape[1]
-    c_at = 2 * k_width
-    u_at, b_at, q_at = c_at + c_width, c_at + 2 * c_width, c_at + 3 * c_width
+    c_at, u_at, b_at = 0, c_width, 2 * c_width
 
     def project(begin, end):
         def body(j, carry):
@@ -391,11 +405,6 @@
     def block(at, j):
         return pl.ds(pl.multiple_of(at + j * lanes, lanes), lanes)
 
-    project(0, c_at)
-    pair_ext[WINDOW : WINDOW + rows, :k_width] = turned(proj_ref[:, :k_width]).astype(bf16)
-    pair_ext[WINDOW : WINDOW + rows, k_width:] = proj_ref[:, k_width : 2 * k_width].astype(bf16)
-    advance(0)
-    start_halo(1)
     project(c_at, b_at)
 
     def carry_body(j, carry):
@@ -405,10 +414,10 @@
         return carry
 
     lax.fori_loop(0, c_width // lanes, carry_body, 0)
-    advance(1)
+    advance(marks[0] + 3)
     start_halo(2)
-    project(b_at, q_at)
-    advance(2)
+    project(b_at, k_at)
+    advance(marks[0] + 4)
     wait_halo(0)
     wait_halo(2)
 
@@ -435,9 +444,16 @@
         return carry
 
     lax.fori_loop(0, c_width // lanes, conv_body, 0)
-    project(q_at, q_at + q_width)
     conv_copy().start()
-    advance(3)
+    settle(1)
+    project(k_at, q_at)
+    keys_at = slice(k_at, k_at + k_width)
+    pair_ext[WINDOW : WINDOW + rows, :k_width] = turned(proj_ref[:, keys_at]).astype(bf16)
+    pair_ext[WINDOW : WINDOW + rows, k_width:] = proj_ref[:, k_at + k_width : q_at].astype(bf16)
+    start_halo(1)
+    advance(marks[1] + 1)
+    project(q_at, width)
+    advance(marks[1] + 2)
 
     def query_body(j, carry):
         cells = turned(proj_ref[:, block(q_at, j)])
@@ -498,20 +514,10 @@
 
     blocks = rows // WINDOW
     lax.fori_loop(0, blocks // 2, attend, 0)
-    advance(4)
+    advance(marks[1] + 4)
     lax.fori_loop(blocks // 2, blocks, attend, 0)
-    advance(5)
     att_copy(blocks - 1).start()
-    y_event(*tail[-1])
-    own_d(1, 1 - c).wait_recv()
-    for t, u in tail:
-        for way in range(2):
-
-            @pl.when(arrives(way, t))
-            def _():
-                d_copy(0, way, t, u, 1 - c).wait_recv()
-                d_copy(1, way, t, u, 1 - c).wait_recv()
-
+    settle(2)
     conv_copy().wait_recv()
     q_mine = pl.ds(pl.multiple_of(x * q_width, q_width), q_width)
     q_yours = pl.ds(pl.multiple_of((1 - x) * q_width, q_width), q_width)
@@ -555,11 +561,11 @@
     conv_copy().wait_send()
     for i in range(blocks):
         att_copy(i).wait_send()
-    for group in range(2):
+    for group in range(3):
         own_d(group, c).wait_send()
     for k in range(TOKEN_CHUNKS):
         x_copy(k).wait_send()
-    for u in proj_units + out_units:
+    for u in range(ends[2]):
         for way in range(2):
 
             @pl.when(has_next[way])
@@ -605,7 +611,7 @@
     doc_cols = jnp.broadcast_to(docs[:, None], (rows, lanes))
     blocks = rows // WINDOW
     dma = pltpu.SemaphoreType.DMA
-    hops = (2, lines - 1, PROJ_UNITS + OUT_UNITS)
+    hops = (2, lines - 1, CONV_UNITS + ATT_UNITS + OUT_UNITS)
     vmem = pl.BlockSpec(memory_space=pltpu.VMEM)
     hbm = pl.BlockSpec(memory_space=pl.ANY)
     smem = pl.BlockSpec(memory_space=pltpu.SMEM)
@@ -633,7 +639,7 @@
             pltpu.VMEM((rows, q_width), bf16),
         ]
         + [dma(hops)] * 8
-        + [dma((2,)), dma((2,)), dma((TOKEN_CHUNKS,)), dma((TOKEN_CHUNKS,)), dma((8,))]
+        + [dma((3,)), dma((3,)), dma((TOKEN_CHUNKS,)), dma((TOKEN_CHUNKS,)), dma((9,))]
         + [dma((3, 2)), dma((3, 2)), dma((2,)), dma((blocks,)), dma((blocks,))],
         compiler_params=pltpu.CompilerParams(
             collective_id=0, has_side_effects=True, vmem_limit_bytes=62 * 1024 * 1024

time: 120 us -> 109 us (0.908)
  Pallas kernels: 111 us -> 100 us
    pallas_call x1, Pallas kernels: 111 us -> 100 us  [fused_layer(): pl.pallas_call(functools.partial(layer_kernel, (lines, rp, ro)), out_shap...]
where the time goes in v3:
time: 109 us; the launch traced here: 108 us
  Pallas kernels  100 us (92%)
  local copies, waits for them, and re-layouts  4.18 us (4%)
  other arithmetic  3.73 us (3%)
    pallas_call x1, Pallas kernels, fused_layer(): pl.pallas_call(functools.partial(layer_kernel, (lines, rp, ro)), out_shap...  100 us
    unnamed x1, local copies, waits for them, and re-layouts  2.67 us

profile of v3, /device:TPU:0, one launch (start us, length us, event | category | flops | bytes accessed | tf_op | source)
XLA Modules:
  0.0 107.9 jit_solution(13014142136066516883)
XLA Ops:
  0.0 0.7 convert_element_type.10
  0.7 0.6 broadcast_in_dim.10.doc_ref
  1.3 0.9 broadcast_in_dim.11.doc_col
  2.2 1.4 %fusion = (f32[768,32]{1,0:T(8,128)S(1)}, f32[768,32]{1,0:T(8,128)S(1)}, f32[768,32]{1,0:T(8,128)S(1)}) fusion(f32[32]{0:T(128)S(1)} %negate_power_fusion, f32[768]{0:T(1024)S(1)} %add_convert_fusion), kind=kLoop, calls=%fused_computation.4 | loop fusion | flops 49152 | bytes 298112 | tf_op jit(solution)/shard_map/neg | solution.py:608
  3.7 1.6 %pad_maximum_fusion = (f32[768,128]{1,0:T(8,128)}, f32[768,128]{1,0:T(8,128)}) fusion(f32[768,32]{1,0:T(8,128)S(1)} %get-tuple-element.7, f32[768,32]{1,0:T(8,128)S(1)} %get-tuple-element.6, f32[768,32]{1,0:T(8,128)S(1)} %get-tuple-element.5), kind=kLoop, calls=%fused_computation.2 | loop fusion | flops 589824 | bytes 1081344 | tf_op jit(solution)/shard_map/concatenate | solution.py:607
  5.3 100.0 %layer.1 = bf16[768,1024]{1,0:T(8,128)(2,1)} custom-call(bf16[768,1024]{1,0:T(8,128)(2,1)} %tok_ref.1, f32[1,2048]{1,0:T(1,128)} %bitcast.2, bf16[256,128]{1,0:T(8,128)(2,1)} %wk_ref.1, bf16[256,128]{1,0:T(8,128)(2,1)} %wv_ref.1, bf16[256,512]{1,0:T(8,128)(2,1)} %wc_ref.1, bf16[256,512]{1,0:T(8,128)(2,1)} %wu_ref.1, bf16[256,512]{1,0:T(8,128)(2,1)} %wb_ref.1, ...), custom_call_target="tpu_custom_call" | custom-call | flops 7247757312 | tf_op jit(solution)/shard_map/layer/pallas_call | solution.py:619
  105.3 2.7 %copy.17 = bf16[768,1024]{1,0:T(8,128)(2,1)} copy(bf16[768,1024]{1,0:T(8,128)(2,1)} %layer.1) | data formatting | bytes 3145728
  (2 shorter events, 0.0 us)
